TPU v7x, 512 devices: a whole 4x4x16 slice. The times are simulated.
512 devices in a mesh: rep: 2 (over z_hi), fs: 32 (over z_lo, y), tp: 8 (over x, core).
Axes of the slice: x: 4, y: 4, z: 16 (z_hi: 2, z_lo: 8; z = z_hi * 8 + z_lo), core: 2. Of those that a mesh axis runs over, the one named last changes fastest.
Arguments:
- tokens: bfloat16 [16384, 2048], P(('rep', 'fs')), may hold values from -6 to 6
- ffn_gate: bfloat16 [2048, 5632], P('fs', 'tp'), may hold values from -0.125 to 0.125
- ffn_up: bfloat16 [2048, 5632], P('fs', 'tp'), may hold values from -0.125 to 0.125
- ffn_down: bfloat16 [5632, 2048], P('tp', 'fs'), may hold values from -0.3125 to 0.3125
- query_proj: bfloat16 [2048, 512], P('fs', 'tp'), may hold values from -0.125 to 0.125
- key_proj: bfloat16 [2048, 512], P('fs', 'tp'), may hold values from -0.125 to 0.125
- value_proj: bfloat16 [2048, 1024], P('fs', 'tp'), may hold values from -0.125 to 0.125
- outgate_proj: bfloat16 [2048, 1024], P('fs', 'tp'), may hold values from -0.125 to 0.125
- output_proj: bfloat16 [1024, 2048], P('tp', 'fs'), may hold values from -0.375 to 0.375
- rank_down: bfloat16 [2048, 16], replicated, may hold values from -0.1875 to 0.1875
- rank_up: bfloat16 [16, 512], replicated, may hold values from -3 to 3
- decay_bias: float32 [512], replicated, may hold values from -0.5 to 8
- head_gain: float32 [1024], replicated, may hold values from 0.1 to 1.9
- norm_gain: float32 [3, 2048], replicated, may hold values from 0.1 to 1.9
- norm_bias: float32 [3, 2048], replicated, may hold values from -2 to 2
Outputs:
- layer_out: bfloat16 [16384, 2048], P(('rep', 'fs'))
All inputs are finite; a program needn't handle non-finite values.
Results may differ from a plain program's by a relative error of at most 0.024.
Values may be sent and summed in bfloat16 or wider, within the bound.
A program may use at most 64 MiB of HBM per device.

v0:
```python
import jax
import jax.numpy as jnp
from jax import lax
from jax.sharding import Mesh
from jax.sharding import PartitionSpec as P

DK = 64
DV = 128
BLOCK = 64
FS = ("fs_0", "fs_1")
REP_FS = ("rep", "fs_0", "fs_1")


EPSILON = 1e-05
HEAD_FLOOR = 1.0
RESIDUAL_SCALE = 2.0**0.5
GATE_SOFTNESS = 16.0


def cut_along(array, dim, count):
    shape = array.shape
    parts = array.reshape(*shape[:dim], count, shape[dim] // count, *shape[dim + 1 :])
    return jnp.moveaxis(parts, dim, 0)


def sum_at_owner(array, axis, dim):
    count = lax.axis_size(axis)
    parts = lax.all_to_all(cut_along(array, dim, count), axis, 0, 0, tiled=True)
    return jnp.sum(parts.astype(jnp.float32), axis=0)


def laid_out(parts, dim):
    shape = list(parts.shape[1:])
    shape[dim] *= parts.shape[0]
    return jnp.moveaxis(parts, 0, dim).reshape(shape)


def from_everyone(array, axis):
    copies = jnp.broadcast_to(array, (lax.axis_size(axis), *array.shape))
    return lax.all_to_all(copies, axis, split_axis=0, concat_axis=0, tiled=True)


def gathered_copies(array, axis, dim):
    return laid_out(from_everyone(array, axis), dim)


def in_one_piece(arrays, axis, dim, along):
    ends, at = ([], 0)
    for a in arrays[:-1]:
        at += a.shape[along]
        ends.append(at)
    both = jnp.concatenate(arrays, axis=along)
    return tuple(jnp.split(lax.all_gather(both, axis, axis=dim, tiled=True), ends, axis=along))


def stacked_from(array, axes, sequence):
    parts = array
    for k in sequence:
        parts = lax.all_gather(parts, axes[k])
    done = sequence[::-1]
    back = [done.index(k) for k in range(len(axes))]
    parts = parts.transpose(*back, *range(len(axes), parts.ndim))
    return parts.reshape(-1, *array.shape)


def gathered_by_axis(array, axes, sequence, dim):
    return laid_out(stacked_from(array, axes, sequence), dim)


def layer_norm(summed, norm_gain, norm_shift):
    centred = summed - jnp.mean(summed, -1, keepdims=True)
    spread = jnp.mean(centred * centred, -1, keepdims=True)
    return (centred * lax.rsqrt(spread + EPSILON) * norm_gain + norm_shift).astype(jnp.bfloat16)


def gla_heads(queries, keys_rows, values, decay_logarithm):
    length, head_count, key_width = queries.shape
    value_width = values.shape[-1]
    block_count = length // BLOCK

    def blocks(array):
        return array.reshape(block_count, BLOCK, head_count, array.shape[-1])

    causal = jnp.tril(jnp.ones((BLOCK, BLOCK), bool))[:, :, None, None]

    def advance(running_state, inputs):
        query_block, key_block, value_block, decay_blk = inputs
        decay_prefix = jnp.cumsum(decay_blk, axis=0)
        spread = decay_prefix[:, None] - decay_prefix[None, :]
        weight = jnp.exp(jnp.where(causal, spread, -jnp.inf))
        scores = jnp.einsum("lshk,lhk,shk->hls", weight, query_block, key_block)
        within = jnp.einsum("hls,shv->lhv", scores, value_block)
        carried_over = jnp.einsum(
            "zew,ewa->zea", query_block * jnp.exp(decay_prefix), running_state
        )
        block_finish = decay_prefix[-1]
        running_state = jnp.exp(block_finish)[:, :, None] * running_state + jnp.einsum(
            "oct,ocy->cty", key_block * jnp.exp(block_finish[None] - decay_prefix), value_block
        )
        return (running_state, within + carried_over)

    initial = jnp.zeros((head_count, key_width, value_width), jnp.float32)
    _, outputs = lax.scan(
        advance,
        initial,
        (blocks(queries), blocks(keys_rows), blocks(values), blocks(decay_logarithm)),
    )
    return outputs.reshape(length, head_count, value_width)


def settle(partial_value, residual_rows, factor, norm_gain, norm_shift):
    portion = sum_at_owner(partial_value.astype(jnp.bfloat16), "tp", 0)
    row_count = portion.shape[0]
    own_rows = lax.dynamic_slice_in_dim(
        residual_rows, lax.axis_index("tp") * row_count, row_count, 0
    )
    normed = layer_norm(
        RESIDUAL_SCALE * own_rows.astype(jnp.float32) + factor * portion, norm_gain, norm_shift
    )
    return gathered_copies(normed, "tp", 0)


def channel_mix(normed, gate_full, up_full, down_full):
    gate_rows = jnp.dot(normed, gate_full, preferred_element_type=jnp.float32)
    up_rows = jnp.dot(normed, up_full, preferred_element_type=jnp.float32)
    hidden = (jax.nn.silu(gate_rows) * up_rows).astype(jnp.bfloat16)
    return jnp.dot(hidden, down_full, preferred_element_type=jnp.float32)


def per_device(
    tokens,
    ffn_gate,
    ffn_up,
    ffn_down,
    query_proj,
    key_proj,
    value_proj,
    outgate_proj,
    output_proj,
    rank_down,
    rank_up,
    decay_bias,
    head_gain,
    norm_gain,
    norm_bias,
):
    row_count = tokens.shape[0]
    gate_full, up_full = in_one_piece((ffn_gate, ffn_up), FS, 0, 1)
    down_full = gathered_by_axis(ffn_down, FS, (0, 1), 1)
    first_partial = channel_mix(tokens, gate_full, up_full, down_full)
    first = settle(first_partial, tokens, 0.5, norm_gain[0], norm_bias[0])
    key_cols = query_proj.shape[1]
    value_cols = value_proj.shape[1]
    query_full, key_full, value_full, outgate_full = in_one_piece(
        (query_proj, key_proj, value_proj, outgate_proj), FS, 0, 1
    )
    joined_full = jnp.concatenate([query_full, key_full, value_full, outgate_full], axis=1)
    projected = jnp.dot(first, joined_full, preferred_element_type=jnp.float32)
    queries = projected[:, :key_cols] * DK ** (-0.5)
    keys_rows = projected[:, key_cols : 2 * key_cols]
    values = projected[:, 2 * key_cols : 2 * key_cols + value_cols]
    gates = projected[:, 2 * key_cols + value_cols :]
    head_count = key_cols // DK
    position = lax.axis_index("tp")
    key_start = position * (head_count * DK)
    value_start = position * (head_count * DV)
    rank_rows = jnp.dot(first, rank_down, preferred_element_type=jnp.float32)
    up_block = lax.dynamic_slice_in_dim(rank_up, key_start, head_count * DK, 1).astype(jnp.float32)
    bias_block = lax.dynamic_slice_in_dim(decay_bias, key_start, head_count * DK, 0)
    decay_source = jnp.dot(rank_rows, up_block) + bias_block
    decay_logarithm = jax.nn.log_sigmoid(decay_source) / GATE_SOFTNESS
    heads_out = gla_heads(
        queries.reshape(row_count, head_count, DK),
        keys_rows.reshape(row_count, head_count, DK),
        values.reshape(row_count, head_count, DV),
        decay_logarithm.reshape(row_count, head_count, DK),
    )
    scaled = heads_out * lax.rsqrt(jnp.mean(heads_out * heads_out, -1, keepdims=True) + HEAD_FLOOR)
    gain_block = lax.dynamic_slice_in_dim(head_gain, value_start, head_count * DV, 0)
    scaled = scaled * gain_block.reshape(head_count, DV)
    mixed = (scaled.reshape(row_count, head_count * DV) * jax.nn.silu(gates)).astype(jnp.bfloat16)
    mixer_partial = jnp.dot(
        mixed, gathered_copies(output_proj, FS, 1), preferred_element_type=jnp.float32
    )
    second = settle(mixer_partial, first, 1.0, norm_gain[1], norm_bias[1])
    third_partial = channel_mix(second, gate_full, up_full, down_full)
    return settle(third_partial, second, 0.5, norm_gain[2], norm_bias[2])


def solution(mesh):
    finer = Mesh(
        mesh.devices.reshape(mesh.shape["rep"], 8, 4, mesh.shape["tp"]),
        ("rep", "fs_0", "fs_1", "tp"),
    )
    return jax.shard_map(
        per_device,
        mesh=finer,
        in_specs=(
            P(REP_FS, None),
            P(FS, "tp"),
            P(FS, "tp"),
            P("tp", FS),
            P(FS, "tp"),
            P(FS, "tp"),
            P(FS, "tp"),
            P(FS, "tp"),
            P("tp", FS),
            P(),
            P(),
            P(),
            P(),
            P(),
            P(),
        ),
        out_specs=P(REP_FS, None),
        check_vma=False,
    )
```

profile of v0, /device:TPU:1, one launch (start us, length us, event | category | flops | bytes accessed | tf_op | source)
XLA Modules:
  0.0 698.8 jit_solution(9261046792770428868)
XLA Ops:
  6.5 50.0 %all-gather.2 = bf16[8,704,64]{1,2,0:T(8,128)(2,1)} all-gather(bf16[1,704,64]{1,2,0:T(8,128)(2,1)} %bitcast.193), channel_id=2, replica_groups=mesh['rep'=2,'fs_0'=8,'fs_1'=4,'tp'=8] {'fs_0'}, dimensions={0}, use_global_device_ids=true | all-gather | bytes 811008 | tf_op jit(solution)/shard_map/all_gather | solution.py:59
  56.6 1.7 pad_maximum_fusion
  58.4 52.3 %all-gather.11.cloned.1.call-done = bf16[32,704,64]{1,2,0:T(8,128)(2,1)} async-done(((bf16[8,704,64]{1,2,0:T(8,128)(2,1)}), bf16[32,704,64]{1,2,0:T(8,128)(2,1)}) %all-gather.11.cloned.1.call-update) | async-done | bytes 2883600 | tf_op jit(solution)/shard_map/all_gather | solution.py:59
  110.7 2.1 copy.30
  112.8 211.7 %all-gather.7.cloned.1.call-done = bf16[2048,1408]{1,0:T(8,128)(2,1)} async-done(((bf16[64,1408]{1,0:T(8,128)(2,1)}), bf16[2048,1408]{1,0:T(8,128)(2,1)}) %all-gather.7.cloned.1.call-update) | async-done | bytes 5767184 | tf_op jit(solution)/shard_map/all_gather | solution.py:53
  324.5 4.1 fusion.33
  328.6 7.8 %convolution_convert_fusion.2 = bf16[256,2048]{1,0:T(8,128)(2,1)} fusion(bf16[704,2048]{0,1:T(8,128)(2,1)S(1)} %bitcast.177, bf16[256,2048]{1,0:T(8,128)(2,1)} %param.17, bf16[2048,1408]{1,0:T(8,128)(2,1)} %all-gather.7.cloned.1.call-done, f32[256,704]{0,1:T(8,128)} %fusion.33), kind=kOutput, calls=%fused_computation.43 | convolution fusion | flops 1478000640 | bytes 8847360 | tf_op jit(solution)/shard_map/dot_general | solution.py:127
  336.4 23.8 %all-to-all-start = ((bf16[8,32,2048]{2,1,0:T(8,128)(2,1)}), bf16[8,32,2048]{2,1,0:T(8,128)(2,1)S(1)}, u32[]{:S(2)}, u32[]{:S(2)}) async-start(bf16[8,32,2048]{2,1,0:T(8,128)(2,1)} %bitcast.187), calls=%async_computation | async-start | bytes 2097152 | tf_op jit(solution)/shard_map/all_to_all | solution.py:28
  361.1 14.1 %all-to-all-done = bf16[8,32,2048]{2,1,0:T(8,128)(2,1)S(1)} async-done(((bf16[8,32,2048]{2,1,0:T(8,128)(2,1)}), bf16[8,32,2048]{2,1,0:T(8,128)(2,1)S(1)}, u32[]{:S(2)}, u32[]{:S(2)}) %all-to-all-start) | async-done | bytes 1048608 | tf_op jit(solution)/shard_map/all_to_all | solution.py:28
  375.4 1.1 fusion.78
  376.5 1.1 multiply_reduce_fusion.2
  377.6 1.0 add_convert_fusion.2
  378.6 1.1 broadcast_in_dim.51
  379.7 4.4 all-to-all-start.1
  385.6 13.5 %all-to-all-done.1 = bf16[8,32,2048]{2,1,0:T(8,128)(2,1)S(1)} async-done(((bf16[8,32,2048]{2,1,0:T(8,128)(2,1)}), bf16[8,32,2048]{2,1,0:T(8,128)(2,1)S(1)}, u32[]{:S(2)}, u32[]{:S(2)}) %all-to-all-start.1) | async-done | bytes 1048608 | tf_op jit(solution)/shard_map/all_to_all | solution.py:40
  399.1 0.9 broadcast_in_dim.54
  400.0 12.0 %all-to-all-start.2 = ((bf16[32,128,64]{1,2,0:T(8,128)(2,1)}), bf16[32,128,64]{1,2,0:T(8,128)(2,1)S(1)}, u32[]{:S(2)}, u32[]{:S(2)}) async-start(bf16[32,128,64]{1,2,0:T(8,128)(2,1)} %broadcast_in_dim.54), calls=%async_computation.2 | async-start | bytes 1048576 | tf_op jit(solution)/shard_map/all_to_all | solution.py:40
  412.0 150.8 %all-gather.9.cloned.1.call-done = bf16[2048,384]{1,0:T(8,128)(2,1)} async-done(((bf16[64,384]{1,0:T(8,128)(2,1)}), bf16[2048,384]{1,0:T(8,128)(2,1)}) %all-gather.9.cloned.1.call-update) | async-done | bytes 1572880 | tf_op jit(solution)/shard_map/all_gather | solution.py:53
  562.8 2.1 fusion.88
  565.0 1.2 fusion.74
  566.4 8.9 %while.13 = (s32[]{:T(128)}, f32[1,64,128]{2,1,0:T(8,128)S(1)}, f32[4,64,1,128]{3,1,2,0:T(8,128)S(1)}, f32[4,64,1,64]{3,1,2,0:T(8,128)S(1)}, f32[4,64,1,64]{3,1,...) while((s32[]{:T(128)}, f32[1,64,128]{2,1,0:T(8,128)S(1)}, ...), condition=%wide.region_5.6_spmd.clone, body=%wide.region_3.5_spmd.clone.sunk | while | flops 5033987 | bytes 1698939 | solution.py:103
  576.1 41.5 %all_to_all.35 = bf16[8,32,2048]{2,1,0:T(8,128)(2,1)S(1)} all-to-all(bf16[8,32,2048]{2,1,0:T(8,128)(2,1)S(1)} %bitcast.173), channel_id=1, replica_groups=mesh['rep'=2,'fs_0'=8,'fs_1'=4,'tp'=8] {'tp'}, dimensions={0} | all-to-all | bytes 2097152 | tf_op jit(solution)/shard_map/all_to_all | solution.py:28
  618.4 18.4 %all_to_all.36 = bf16[8,32,2048]{2,1,0:T(8,128)(2,1)S(1)} all-to-all(bf16[8,32,2048]{2,1,0:T(8,128)(2,1)S(1)} %broadcast_in_dim.55), channel_id=1, replica_groups=mesh['rep'=2,'fs_0'=8,'fs_1'=4,'tp'=8] {'tp'}, dimensions={0} | all-to-all | bytes 2097152 | tf_op jit(solution)/shard_map/all_to_all | solution.py:40
  636.8 1.0 copy-done.3
  637.8 4.5 fusion.29
  642.3 7.7 %convolution_convert_fusion.1 = bf16[256,2048]{1,0:T(8,128)(2,1)} fusion(bf16[704,2048]{0,1:T(8,128)(2,1)S(1)} %bitcast.178, bf16[256,2048]{1,0:T(8,128)(2,1)} %bitcast.182, bf16[2048,1408]{1,0:T(8,128)(2,1)} %all-gather.7.cloned.1.call-done, f32[256,704]{0,1:T(8,128)} %fusion.29), kind=kOutput, calls=%fused_computation.42 | convolution fusion | flops 1478000640 | bytes 8847360 | tf_op jit(solution)/shard_map/dot_general | solution.py:127
  650.0 19.4 %all_to_all.37 = bf16[8,32,2048]{2,1,0:T(8,128)(2,1)S(1)} all-to-all(bf16[8,32,2048]{2,1,0:T(8,128)(2,1)} %bitcast.188), channel_id=1, replica_groups=mesh['rep'=2,'fs_0'=8,'fs_1'=4,'tp'=8] {'tp'}, dimensions={0} | all-to-all | bytes 2097152 | tf_op jit(solution)/shard_map/all_to_all | solution.py:28
  669.5 1.1 fusion.79
  670.6 1.1 multiply_reduce_fusion
  671.7 1.0 add_convert_fusion
  672.9 18.4 %all_to_all.38 = bf16[8,32,2048]{2,1,0:T(8,128)(2,1)S(1)} all-to-all(bf16[8,32,2048]{2,1,0:T(8,128)(2,1)S(1)} %broadcast_in_dim.56), channel_id=1, replica_groups=mesh['rep'=2,'fs_0'=8,'fs_1'=4,'tp'=8] {'tp'}, dimensions={0} | all-to-all | bytes 2097152 | tf_op jit(solution)/shard_map/all_to_all | solution.py:40
  691.3 1.0 copy.54
  (105 shorter events, 13.2 us)
Async XLA Ops:
  6.5 558.5 %copy-start = (bf16[2048,16]{0,1:T(8,128)(2,1)S(1)}, bf16[2048,16]{0,1:T(8,128)(2,1)}, u32[]{:S(2)}) copy-start(bf16[2048,16]{0,1:T(8,128)(2,1)} %param.26) | copy-start | bytes 196612
  6.5 104.1 %all-gather.11.cloned.1.call-start = ((), (), s32[]{:S(2)}) async-start(), calls=%async_computation.9 | async-start | bytes 3932160 | tf_op jit(solution)/shard_map/all_gather | solution.py:59
  56.6 267.9 %all-gather.7.cloned.1.call-start = ((), (), s32[]{:S(2)}) async-start(), calls=%async_computation.7 | async-start | bytes 5947392 | tf_op jit(solution)/shard_map/all_gather | solution.py:53
  112.8 215.8 %copy-start.1 = (bf16[8,4,704,64]{2,3,1,0:T(8,128)(2,1)}, bf16[8,4,704,64]{2,3,1,0:T(8,128)(2,1)S(1)}, u32[]{:S(2)}) copy-start(bf16[8,4,704,64]{2,3,1,0:T(8,128)(2,1)S(1)} %copy.30) | copy-start | bytes 8650756
  328.6 31.7 %copy-start.6 = (bf16[64,128]{1,0:T(8,128)(2,1)S(1)}, bf16[64,128]{1,0:T(8,128)(2,1)}, u32[]{:S(2)}) copy-start(bf16[64,128]{1,0:T(8,128)(2,1)} %param.24) | copy-start | bytes 49156
  328.6 31.7 %copy-start.7 = (bf16[64,128]{1,0:T(8,128)(2,1)S(1)}, bf16[64,128]{1,0:T(8,128)(2,1)}, u32[]{:S(2)}) copy-start(bf16[64,128]{1,0:T(8,128)(2,1)} %param.23) | copy-start | bytes 49156
  328.6 31.7 %copy-start.8 = (bf16[64,64]{1,0:T(8,128)(2,1)S(1)}, bf16[64,64]{1,0:T(8,128)(2,1)}, u32[]{:S(2)}) copy-start(bf16[64,64]{1,0:T(8,128)(2,1)} %param.22) | copy-start | bytes 24580
  328.6 31.7 %copy-start.9 = (bf16[64,64]{1,0:T(8,128)(2,1)S(1)}, bf16[64,64]{1,0:T(8,128)(2,1)}, u32[]{:S(2)}) copy-start(bf16[64,64]{1,0:T(8,128)(2,1)} %param.21) | copy-start | bytes 24580
  328.6 32.4 %copy-start.4 = (f32[3,2048]{1,0:T(4,128)S(1)}, f32[3,2048]{1,0:T(4,128)}, u32[]{:S(2)}) copy-start(f32[3,2048]{1,0:T(4,128)} %param.31) | copy-start | bytes 73732
  328.6 32.5 %copy-start.5 = (f32[3,2048]{1,0:T(4,128)S(1)}, f32[3,2048]{1,0:T(4,128)}, u32[]{:S(2)}) copy-start(f32[3,2048]{1,0:T(4,128)} %param.30) | copy-start | bytes 73732
  336.4 38.8 %all-to-all-start = ((bf16[8,32,2048]{2,1,0:T(8,128)(2,1)}), bf16[8,32,2048]{2,1,0:T(8,128)(2,1)S(1)}, u32[]{:S(2)}, u32[]{:S(2)}) async-start(bf16[8,32,2048]{2,1,0:T(8,128)(2,1)} %bitcast.187), calls=%async_computation | async-start | bytes 2097152 | tf_op jit(solution)/shard_map/all_to_all | solution.py:28
  360.3 38.9 %copy-start.10 = (bf16[128,64]{0,1:T(8,128)(2,1)S(1)}, bf16[128,64]{0,1:T(8,128)(2,1)}, u32[]{:S(2)}) copy-start(bf16[128,64]{0,1:T(8,128)(2,1)} %param.25) | copy-start | bytes 49156
  360.3 202.5 %all-gather.9.cloned.1.call-start = ((), (), s32[]{:S(2)}) async-start(), calls=%async_computation.8 | async-start | bytes 1622016 | tf_op jit(solution)/shard_map/all_gather | solution.py:53
  379.7 19.4 %all-to-all-start.1 = ((bf16[8,32,2048]{2,1,0:T(8,128)(2,1)}), bf16[8,32,2048]{2,1,0:T(8,128)(2,1)S(1)}, u32[]{:S(2)}, u32[]{:S(2)}) async-start(bf16[8,32,2048]{2,1,0:T(8,128)(2,1)} %broadcast_in_dim.51), calls=%async_computation.1 | async-start | bytes 2097152 | tf_op jit(solution)/shard_map/all_to_all | solution.py:40
  400.0 175.6 %all-to-all-start.2 = ((bf16[32,128,64]{1,2,0:T(8,128)(2,1)}), bf16[32,128,64]{1,2,0:T(8,128)(2,1)S(1)}, u32[]{:S(2)}, u32[]{:S(2)}) async-start(bf16[32,128,64]{1,2,0:T(8,128)(2,1)} %broadcast_in_dim.54), calls=%async_computation.2 | async-start | bytes 1048576 | tf_op jit(solution)/shard_map/all_to_all | solution.py:40
  636.8 1.0 copy-start.3
  636.8 5.5 copy-start.2
Sparse Core Ops, SparseCore 0:
  56.7 53.8 all-gather.10
  112.7 211.6 all-gather.6
  363.2 199.6 all-gather.8
where the time goes:
time: 700 us; the launch traced here: 699 us
  waiting for transfers between devices  442 us (63%)
  blocking collectives  148 us (21%)
  starting transfers between devices  40.3 us (6%)
  matrix products  33 us (5%)
  other arithmetic  13.5 us (2%)
  between operations  13.4 us (2%)
  local copies, waits for them, and re-layouts  8.18 us (1%)
    all_gather x2, waiting for transfers between devices, in_one_piece(): lax.all_gather(both, axis, axis=dim, tiled=True)  362 us
    all_to_all x2, blocking collectives, sum_at_owner(): parts = lax.all_to_all(cut_along(array, dim, count), axis, 0, 0, tiled=True)  61 us
    all_gather x1, waiting for transfers between devices, stacked_from(): parts = lax.all_gather(parts, axes[k])  52.3 us
    all_gather x1, blocking collectives, stacked_from(): parts = lax.all_gather(parts, axes[k])  50 us
    all_to_all x2, blocking collectives, from_everyone(): return lax.all_to_all(copies, axis, split_axis=0, concat_axis=0, tiled=True)  36.8 us
    all_to_all x1, starting transfers between devices, sum_at_owner(): parts = lax.all_to_all(cut_along(array, dim, count), axis, 0, 0, tiled=True)  23.8 us
    all_to_all x2, starting transfers between devices, from_everyone(): return lax.all_to_all(copies, axis, split_axis=0, concat_axis=0, tiled=True)  16.4 us
    dot_general x2, matrix products, channel_mix(): return jnp.dot(hidden, down_full, preferred_element_type=jnp.float32)  15.5 us
  transfers between devices with their start and end apart: 6, of which 5 were waited for; matrix products, arithmetic and copies ran while one was open for 3% of the time, Pallas kernels for 0%

commit v1 on v0

v1 whole, which is shorter than its diff:
```python
import functools
import heapq

import jax
import jax.numpy as jnp
from jax import lax
from jax.experimental import pallas as pl
from jax.experimental.pallas import tpu as pltpu
from jax.sharding import Mesh
from jax.sharding import PartitionSpec as P

DK = 64
DV = 128
FS = ("fs_0", "fs_1")
REP_FS = ("rep", "fs_0", "fs_1")
NZ, NY, NX = 8, 4, 4
ROWS = 256
D = 2048
SHARD = 64
COLS = 256
OWN = 32

EPSILON = 1e-05
HEAD_FLOOR = 1.0
RESIDUAL_SCALE = 2.0**0.5
GATE_SOFTNESS = 16.0

MESH = pl.DeviceIdType.MESH
F32 = jnp.float32
BF16 = jnp.bfloat16
LINKS = ("z+", "z-", "y+", "y-")
WIDTHS = ((7, 4), (3, 3), (2, 2))
NEAREST = (0, 1, -1, 2, -2, 3, -3, 4)


def gather_items():
    items = []

    def add(chunk, part, link, slot, half, depth):
        dz, dy = slot
        lands = {"z+": (dz - 1, dy), "z-": (dz + 1, dy), "y+": (dz, dy - 1), "y-": (dz, dy + 1)}[link]
        size = WIDTHS[chunk][part] * (1.0 if half is None else 0.5)
        items.append((chunk, part, link, slot, half, lands, depth, size))

    def along_z(chunk, part, dy, more):
        for s in range(4):
            add(chunk, part, "z+", (-s, dy), None if s < 3 else 0, 4 - s + more)
            add(chunk, part, "z-", (s, dy), None if s < 3 else 1, 4 - s + more)

    def along_y(chunk, part, dz, more):
        add(chunk, part, "y+", (dz, 0), None, 2 + more)
        add(chunk, part, "y-", (dz, 0), None, 2 + more)
        add(chunk, part, "y+", (dz, -1), 0, 1 + more)
        add(chunk, part, "y-", (dz, 1), 1, 1 + more)

    for chunk in range(len(WIDTHS)):
        along_z(chunk, 0, 0, 2)
        for dz in NEAREST:
            along_y(chunk, 0, dz, 0)
        along_y(chunk, 1, 0, 4)
        for dy in (0, 1, -1, 2):
            along_z(chunk, 1, dy, 0)
    return items


def spot(slot):
    return (slot[0] % NZ, slot[1] % NY)


def gather_order(backlog=2.0, tile_us=0.352, fixed=0.05, hop=2.2):
    items = gather_items()
    held = {(c, p, (0, 0)): {0, 1} for c in range(len(WIDTHS)) for p in (0, 1)}
    waiting = list(range(len(items)))
    ready = {link: [] for link in LINKS}
    free = {link: 0.0 for link in LINKS}
    order, flying = [], []

    def step(now):
        left = []
        for i in waiting:
            chunk, part, link, slot, half = items[i][:5]
            have = held.get((chunk, part, spot(slot)), set())
            if have >= ({0, 1} if half is None else {half}):
                ready[link].append(i)
            else:
                left.append(i)
        waiting[:] = left
        for link in LINKS:
            ready[link].sort(key=lambda i: (items[i][0], -items[i][6], i))
            while ready[link] and free[link] - now < backlog:
                i = ready[link].pop(0)
                free[link] = max(now, free[link]) + items[i][7] * tile_us + fixed
                heapq.heappush(flying, (free[link] + hop, i))
                order.append((now, "send", i))

    step(0.0)
    while flying:
        now, i = heapq.heappop(flying)
        chunk, part, _, _, half, lands = items[i][:6]
        held.setdefault((chunk, part, spot(lands)), set()).update({0, 1} if half is None else {half})
        order.append((now, "land", i))
        step(now)
    return items, order


def dot_nt(a, b):
    return lax.dot_general(a, b, (((1,), (1,)), ((), ())), preferred_element_type=F32)


def dot_nn(a, b, precision=None):
    return lax.dot_general(a, b, (((1,), (0,)), ((), ())), preferred_element_type=F32, precision=precision)


def silu(v):
    return v / (1.0 + jnp.exp(-v))


def boundary(prefix, m):
    if m >= 4:
        parts = prefix.reshape(ROWS // (2 * m), 2 * m, DK)
        edge = jnp.broadcast_to(parts[:, m - 1 : m, :], parts.shape)
        return edge.reshape(ROWS, DK)
    parts = prefix.reshape(ROWS // 8, 8, DK)
    row = lax.broadcasted_iota(jnp.int32, parts.shape, 1)
    edge = jnp.broadcast_to(parts[:, 8 - m - 1 : 8 - m, :], parts.shape)
    for at in range(8 - 4 * m, -1, -2 * m):
        edge = jnp.where(row < at + 2 * m, jnp.broadcast_to(parts[:, at + m - 1 : at + m, :], parts.shape), edge)
    return edge.reshape(ROWS, DK)


def head_out(q, k, v, log_decay):
    row = lax.broadcasted_iota(jnp.int32, (ROWS, ROWS), 0)
    col = lax.broadcasted_iota(jnp.int32, (ROWS, ROWS), 1)
    prefix = dot_nn((col <= row).astype(F32), log_decay, lax.Precision.HIGHEST)
    apart = row ^ col
    scores = jnp.where(row == col, jnp.sum(q * k, axis=1, keepdims=True), 0.0)
    m = ROWS // 2
    while m:
        fade = jnp.exp(-jnp.abs(prefix - boundary(prefix, m)))
        level = dot_nt((q * fade).astype(BF16), (k * fade).astype(BF16))
        scores = jnp.where((row > col) & (apart >= m) & (apart < 2 * m), level, scores)
        m //= 2
    return dot_nn(scores.astype(BF16), v.astype(BF16))


def layer_kernel(items, order, *refs):
    (tok, ga, gb, da, db, qa, qb, rank_down, rank_up, bias, head_gain, norm_gain, norm_bias) = refs[:13]
    out = refs[13]
    (GA, GB, DA, DB, QA, QB, acc_a, acc_b, hid, first, second, mixed, sendbuf, pairbuf, xsend, xrecv, tot) = refs[14:31]
    (put_sem, get_sem, own_sem, pair_s, pair_r, x_s, x_r, ag_s, ag_r) = refs[31:]
    shards = ((ga, gb), (da, db), (qa, qb))
    bufs = ((GA, GB), (DA, DB), (QA, QB))

    rep, zl, y, tp = (lax.axis_index(a) for a in ("rep", "fs_0", "fs_1", "tp"))
    zg = rep * NZ + zl
    x, c = tp // 2, lax.rem(tp, 2)
    other = 1 - c

    def at_z(step):
        g = lax.rem(zg + step + 16, 16)
        return (g // NZ, lax.rem(g, NZ), y, tp)

    def at_y(step):
        return (rep, zl, lax.rem(y + step + NY, NY), tp)

    def at_x(step):
        return (rep, zl, y, lax.rem(x + step + NX, NX) * 2 + c)

    partner = (rep, zl, y, x * 2 + other)
    where = {"z+": at_z(1), "z-": at_z(-1), "y+": at_y(1), "y-": at_y(-1)}
    xs = [at_x(s) for s in (1, 2, 3)]
    from_x = [lax.rem(x - s + NX, NX) for s in (1, 2, 3)]
    z_at = {k: lax.rem(zl + k, NZ) for k in range(NZ)}
    y_at = {k: lax.rem(y + k, NY) for k in range(NY)}

    barrier = pltpu.get_barrier_semaphore()
    friends = list(where.values()) + xs + [partner]
    for friend in friends:
        pl.semaphore_signal(barrier, inc=1, device_id=friend, device_id_type=MESH)
    owns = []
    for k in range(3):
        for p in range(2):
            copy = pltpu.make_async_copy(shards[k][p], bufs[k][p].at[zl, y], own_sem.at[2 * k + p])
            copy.start()
            owns.append(copy)
    pl.semaphore_wait(barrier, len(friends))

    def place(chunk, part, slot, half):
        dz, dy = spot(slot)
        buf = bufs[chunk][part]
        if half is None:
            return buf.at[z_at[dz], y_at[dy]]
        return buf.at[z_at[dz], y_at[dy], pl.ds(32 * half, 32)]

    def item_copy(i, landing):
        chunk, part, link, slot, half, lands = items[i][:6]
        here = place(chunk, part, lands if landing else slot, half)
        src = here
        if not landing and spot(slot) == (0, 0):
            src = shards[chunk][part] if half is None else shards[chunk][part].at[pl.ds(32 * half, 32)]
        return pltpu.make_async_remote_copy(
            src_ref=src, dst_ref=here, send_sem=put_sem.at[i], recv_sem=get_sem.at[i],
            device_id=where[link], device_id_type=MESH)

    def near(i):
        return lax.rem(zl + ((i + 1) // 2) * (2 * lax.rem(i, 2) - 1) + NZ, NZ)

    def gate_up(source, lo, hi):
        def step(i, carry):
            zi = near(i)
            a = source[:, pl.ds(pl.multiple_of(zi * COLS, COLS), COLS)]
            acc_a[...] += dot_nn(a, GA[zi].reshape(COLS, 896))
            acc_b[...] += dot_nn(a, GB[zi].reshape(COLS, 512))
            return carry
        lax.fori_loop(lo, hi, step, 0)

    def clear():
        acc_a[...] = jnp.zeros_like(acc_a)
        acc_b[...] = jnp.zeros_like(acc_b)

    def hidden():
        hid[:, 0:256] = (silu(acc_a[:, 0:256]) * acc_a[:, 640:896]).astype(BF16)
        hid[:, 256:640] = (silu(acc_a[:, 256:640]) * acc_b[:, 0:384]).astype(BF16)
        last = acc_b[:, 384:512]
        lane = lax.broadcasted_iota(jnp.int32, last.shape, 1)
        mixed_last = silu(last) * pltpu.roll(last, 64, 1)
        hid[:, 640:768] = jnp.where(lane < 64, mixed_last, 0.0).astype(BF16)

    def down_part(zi):
        return dot_nt(hid[:, :384], DA[zi].reshape(COLS, 384)) + dot_nt(hid[:, 384:], DB[zi].reshape(COLS, 384))

    def output_part(zi):
        return dot_nt(mixed[...], QB[zi][:, :, 128:].reshape(COLS, 128))

    def pair_copy(zi):
        return pltpu.make_async_remote_copy(
            src_ref=sendbuf.at[zi, other], dst_ref=pairbuf.at[zi], send_sem=pair_s.at[zi], recv_sem=pair_r.at[zi],
            device_id=partner, device_id_type=MESH)

    def x_copy(zi, s):
        return pltpu.make_async_remote_copy(
            src_ref=xsend.at[zi, lax.rem(x + s + 1, NX)], dst_ref=xrecv.at[s, zi],
            send_sem=x_s.at[s, zi], recv_sem=x_r.at[s, zi], device_id=xs[s], device_id_type=MESH)

    def front(part, zi):
        value = part(zi)
        for t in range(8):
            sendbuf[zi, t % 2, t // 2] = value[t * OWN : (t + 1) * OWN].astype(BF16)
        pair_copy(zi).start()

    def middle(zi):
        pair_copy(zi).wait_recv()
        xsend[zi] = (sendbuf[zi, c].astype(F32) + pairbuf[zi].astype(F32)).astype(BF16)
        for s in (1, 0, 2):
            x_copy(zi, s).start()

    row0 = pl.multiple_of(tp * OWN, OWN)

    def settle(source, target, factor, which):
        def wait(zi, carry):
            for s in range(3):
                x_copy(zi, s).wait_recv()
            return carry
        lax.fori_loop(0, NZ, wait, 0)
        own = source[pl.ds(row0, OWN), :].astype(F32)
        total = jnp.zeros((OWN, 1), F32)
        for zi in range(NZ):
            part = sendbuf[zi, c, x].astype(F32) + pairbuf[zi, x].astype(F32)
            for s in range(3):
                part = part + xrecv[s, zi].astype(F32)
            part = RESIDUAL_SCALE * own[:, zi * COLS : (zi + 1) * COLS] + factor * part
            tot[:, zi * COLS : (zi + 1) * COLS] = part
            total = total + jnp.sum(part, axis=1, keepdims=True)
        centred = tot[...] - total * (1.0 / D)
        spread = jnp.mean(centred * centred, axis=1, keepdims=True)
        normed = centred * lax.rsqrt(spread + EPSILON) * norm_gain[which : which + 1, :] + norm_bias[which : which + 1, :]
        target[pl.ds(row0, OWN), :] = normed.astype(BF16)

    def rows_of(target, xx, cc, half):
        start = pl.multiple_of((xx * 2 + cc) * OWN + 16 * half, 16)
        return target.at[pl.ds(start, 16)]

    def ag_copy(target, k, half, xx, cc, to):
        ref = rows_of(target, xx, cc, half)
        return pltpu.make_async_remote_copy(
            src_ref=ref, dst_ref=ref, send_sem=ag_s.at[k, half], recv_sem=ag_r.at[k, half],
            device_id=to, device_id_type=MESH)

    def spread_out(target):
        for half in range(2):
            for s in (1, 0, 2):
                ag_copy(target, s, half, x, c, xs[s]).start()
        for half in range(2):
            ag_copy(target, 3, half, x, c, partner).start()

    def pass_on(target, s, half):
        ag_copy(target, s, half, from_x[s], c, xs[s]).wait_recv()
        ag_copy(target, 4 + s, half, from_x[s], c, partner).start()

    def gathered(target):
        for half in range(2):
            ag_copy(target, 3, half, x, other, partner).wait_recv()
        for half in range(2):
            for s in range(3):
                ag_copy(target, 4 + s, half, from_x[s], other, partner).wait_recv()

    def drain(target):
        def wait(zi, carry):
            pair_copy(zi).wait_send()
            for s in range(3):
                x_copy(zi, s).wait_send()
            return carry
        lax.fori_loop(0, NZ, wait, 0)
        for half in range(2):
            for s in range(3):
                ag_copy(target, s, half, x, c, xs[s]).wait_send()
                ag_copy(target, 4 + s, half, from_x[s], c, partner).wait_send()
            ag_copy(target, 3, half, x, c, partner).wait_send()

    held = {}
    done_groups = [[], [], []]
    state = {"gate": 0, "fronts": [], "middles": []}
    end_of = [max(t for t, kind, i in order if kind == "land" and items[i][0] == k) for k in range(3)]
    steps = [(t, 0, kind, i) for t, kind, i in order]
    steps += [(end_of[1] + 4.5, 1, "settle", 0)]
    steps += [(end_of[1] + 4.6, 2, "spread", 0)]
    at = end_of[1] + 8.0
    for half in range(2):
        for s in (0, 2, 1):
            steps.append((at + 1.5 * half + (0.7 if s == 1 else 0.0), 3, "pass", (s, half)))
    steps.sort(key=lambda e: e[:2])
    clear()

    def flush_middles(keep):
        while len(state["middles"]) > keep:
            middle(state["middles"].pop(0))

    for now, _, kind, what in steps:
        if kind == "send":
            item_copy(what, False).start()
        elif kind == "land":
            item_copy(what, True).wait_recv()
            chunk, part, _, _, half, lands = items[what][:6]
            key = (chunk, spot(lands)[0])
            held[key] = held.get(key, 0.0) + (1.0 if half is None else 0.5)
            full = 6.0 if spot(lands)[0] == 0 else 8.0
            if held[key] == full:
                done_groups[chunk].append(spot(lands)[0])
                if chunk == 0 and spot(lands)[0] == 0:
                    for copy in owns:
                        copy.wait()
            if chunk == 0 and {spot((k, 0))[0] for k in NEAREST[:5]} <= set(done_groups[0]) and state["gate"] == 0:
                gate_up(tok, 0, 5)
                state["gate"] = 5
            if chunk == 0 and len(done_groups[0]) == NZ and state["gate"] == 5:
                gate_up(tok, 5, 8)
                hidden()
                state["gate"] = 8
            if state["gate"] == 8:
                for k in done_groups[1]:
                    if k not in state["fronts"]:
                        state["fronts"].append(k)
                        front(down_part, z_at[k])
                        state["middles"].append(z_at[k])
                        flush_middles(2)
                if len(state["fronts"]) == NZ:
                    flush_middles(0)
        elif kind == "settle":
            settle(tok, first, 0.5, 0)
        elif kind == "spread":
            spread_out(first)
        else:
            pass_on(first, *what)
    gathered(first)

    rows = first[...]
    proj = dot_nn(rows, QA[...].reshape(D, 256))
    gates = dot_nn(rows, QB[:, :, :, :128].reshape(D, 128))
    ranks = dot_nt(rows, rank_down[...])
    source = dot_nn(ranks, rank_up[...], lax.Precision.HIGHEST) + bias[...]
    log_decay = (jnp.minimum(source, 0.0) - jnp.log1p(jnp.exp(-jnp.abs(source)))) * (1.0 / GATE_SOFTNESS)
    heads = head_out(proj[:, :DK] * DK**-0.5, proj[:, DK : 2 * DK], proj[:, 2 * DK :], log_decay)
    scale = lax.rsqrt(jnp.mean(heads * heads, axis=1, keepdims=True) + HEAD_FLOOR)
    mixed[...] = (heads * scale * head_gain[...] * silu(gates)).astype(BF16)
    drain(first)

    def reduce_scatter(part, lag):
        def fronts(zi, carry):
            front(part, zi)
            return carry

        def both(zi, carry):
            front(part, zi)
            middle(zi - lag)
            return carry

        def middles(zi, carry):
            middle(zi)
            return carry
        lax.fori_loop(0, lag, fronts, 0)
        lax.fori_loop(lag, NZ, both, 0)
        lax.fori_loop(NZ - lag, NZ, middles, 0)

    def all_rows(target):
        spread_out(target)
        for half in range(2):
            for s in (0, 2, 1):
                pass_on(target, s, half)
        gathered(target)

    reduce_scatter(output_part, 3)
    settle(first, second, 1.0, 1)
    all_rows(second)

    clear()
    gate_up(second, 0, 8)
    hidden()
    drain(second)
    reduce_scatter(down_part, 3)
    settle(second, out, 0.5, 2)
    all_rows(out)
    drain(out)

    for t, kind, i in order:
        if kind == "send":
            item_copy(i, False).wait_send()


def per_device(
    tokens, ffn_gate, ffn_up, ffn_down, query_proj, key_proj, value_proj, outgate_proj, output_proj,
    rank_down, rank_up, decay_bias, head_gain, norm_gain, norm_bias,
):
    tp = lax.axis_index("tp")
    ga = jnp.concatenate([ffn_gate[:, :640], ffn_up[:, :256]], axis=1)
    gb = jnp.concatenate([ffn_up[:, 256:640], ffn_gate[:, 640:], ffn_up[:, 640:]], axis=1)
    down = jnp.pad(ffn_down.T, ((0, 0), (0, 64)))
    da, db = down[:, :384], down[:, 384:]
    qa = jnp.concatenate([query_proj, key_proj, value_proj], axis=1)
    qb = jnp.concatenate([outgate_proj, output_proj.T], axis=1)
    up_block = lax.dynamic_slice_in_dim(rank_up, tp * DK, DK, 1).astype(F32)
    bias_block = lax.dynamic_slice_in_dim(decay_bias, tp * DK, DK, 0).reshape(1, DK)
    gain_block = lax.dynamic_slice_in_dim(head_gain, tp * DV, DV, 0).reshape(1, DV)
    items, order = gather_order()
    count = len(items)
    dma = pltpu.SemaphoreType.DMA
    vmem = pl.BlockSpec(memory_space=pltpu.VMEM)
    scratch = [
        pltpu.VMEM((NZ, NY, SHARD, 896), BF16),
        pltpu.VMEM((NZ, NY, SHARD, 512), BF16),
        pltpu.VMEM((NZ, NY, SHARD, 384), BF16),
        pltpu.VMEM((NZ, NY, SHARD, 384), BF16),
        pltpu.VMEM((NZ, NY, SHARD, 256), BF16),
        pltpu.VMEM((NZ, NY, SHARD, 256), BF16),
        pltpu.VMEM((ROWS, 896), F32),
        pltpu.VMEM((ROWS, 512), F32),
        pltpu.VMEM((ROWS, 768), BF16),
        pltpu.VMEM((ROWS, D), BF16),
        pltpu.VMEM((ROWS, D), BF16),
        pltpu.VMEM((ROWS, DV), BF16),
        pltpu.VMEM((NZ, 2, NX, OWN, COLS), BF16),
        pltpu.VMEM((NZ, NX, OWN, COLS), BF16),
        pltpu.VMEM((NZ, NX, OWN, COLS), BF16),
        pltpu.VMEM((3, NZ, OWN, COLS), BF16),
        pltpu.VMEM((OWN, D), F32),
        dma((count,)), dma((count,)), dma((6,)),
        dma((NZ,)), dma((NZ,)), dma((3, NZ)), dma((3, NZ)), dma((7, 2)), dma((7, 2)),
    ]
    return pl.pallas_call(
        functools.partial(layer_kernel, items, order),
        out_shape=jax.ShapeDtypeStruct((ROWS, D), BF16),
        in_specs=[vmem] * 13,
        out_specs=vmem,
        scratch_shapes=scratch,
        compiler_params=pltpu.CompilerParams(
            collective_id=0, has_side_effects=True, vmem_limit_bytes=60 * 1024 * 1024),
        name="layer",
    )(tokens, ga, gb, da, db, qa, qb, rank_down.T, up_block, bias_block, gain_block, norm_gain, norm_bias)


def solution(mesh):
    finer = Mesh(
        mesh.devices.reshape(mesh.shape["rep"], NZ, NY, mesh.shape["tp"]),
        ("rep", "fs_0", "fs_1", "tp"),
    )
    return jax.shard_map(
        per_device,
        mesh=finer,
        in_specs=(
            P(REP_FS, None), P(FS, "tp"), P(FS, "tp"), P("tp", FS), P(FS, "tp"), P(FS, "tp"), P(FS, "tp"),
            P(FS, "tp"), P("tp", FS), P(), P(), P(), P(), P(), P(),
        ),
        out_specs=P(REP_FS, None),
        check_vma=False,
    )
```

time: 700 us -> 153 us (0.22)
  waiting for transfers between devices: 442 us -> 0 us
  blocking collectives: 148 us -> 0 us
  Pallas kernels: 0 us -> 142 us
  starting transfers between devices: 40.3 us -> 0 us
  matrix products: 33 us -> 0 us
  between operations: 13.4 us -> 0.04 us
  other arithmetic: 13.5 us -> 3.42 us
    all_gather x3 -> x0, waiting for transfers between devices: 415 us -> none  [the longest x2 362 us: in_one_piece(): lax.all_gather(both, axis, axis=dim, tiled=True)]
    pallas_call x0 -> x1, Pallas kernels: none -> 142 us  [per_device(): pl.pallas_call(functools.partial(layer_kernel, items, order), out_shape=j...]
    all_to_all x4 -> x0, blocking collectives: 97.8 us -> none  [the longest x2 61 us: sum_at_owner(): parts = lax.all_to_all(cut_along(array, dim, count), axis, 0, 0, tiled=True)]
    all_gather x1 -> x0, blocking collectives: 50 us -> none  [stacked_from(): parts = lax.all_gather(parts, axes[k])]
    all_to_all x3 -> x0, starting transfers between devices: 40.2 us -> none  [the longest x1 23.8 us: sum_at_owner(): parts = lax.all_to_all(cut_along(array, dim, count), axis, 0, 0, tiled=True)]
    dot_general x23 -> x0, matrix products: 33 us -> none  [the longest x2 15.5 us: channel_mix(): return jnp.dot(hidden, down_full, preferred_element_type=jnp.float32)]
    all_to_all x3 -> x0, waiting for transfers between devices: 27.6 us -> none  [the longest x1 14.1 us: sum_at_owner(): parts = lax.all_to_all(cut_along(array, dim, count), axis, 0, 0, tiled=True)]
  transfers between devices with their start and end apart: 6 -> 0, of which waited for: 5 -> 0; matrix products, arithmetic and copies ran while one was open for 3% -> 0% of each run, Pallas kernels for 0% -> 0%
where the time goes in v1:
time: 153 us
  Pallas kernels  142 us (93%)
  local copies, waits for them, and re-layouts  7.62 us (5%)
  other arithmetic  3.42 us (2%)
    pallas_call x1, Pallas kernels, per_device(): pl.pallas_call(functools.partial(layer_kernel, items, order), out_shape=j...  142 us
    unnamed x15, local copies, waits for them, and re-layouts  3.32 us

profile of v1, /device:TPU:1, one launch (start us, length us, event | category | flops | bytes accessed | tf_op | source)
XLA Modules:
  0.0 152.6 jit_solution(17193431806214844442)
XLA Ops:
  0.0 0.0 copy-start
  0.0 0.7 copy-done
  0.7 0.6 dynamic-slice_bitcast_fusion.refs_10_
  1.3 1.3 dynamic-slice_bitcast_fusion.1.refs_9_
  2.6 1.4 dynamic-slice_convert_fusion.refs_8_
  4.0 0.0 slice-start
  4.0 0.0 slice-start.2
  4.0 0.0 slice-start.4
  4.0 0.7 slice-done
  4.7 0.0 slice-done.2
  4.7 0.1 slice-done.4
  4.8 0.0 copy-start.2
  4.8 0.0 copy-start.3
  4.8 0.0 copy-start.4
  4.8 0.0 copy-start.5
  4.8 0.0 copy-start.6
  4.8 0.7 pad_maximum_fusion.1.refs_2_
  5.5 0.0 copy-done.2
  5.5 0.0 copy-done.3
  5.5 0.0 copy-done.4
  5.6 0.0 copy-done.5
  5.6 0.0 copy-done.6
  5.6 0.7 pad_maximum_fusion.2
  6.3 0.0 slice-start.1
  6.3 0.0 slice-start.3
  6.3 0.9 slice-done.1
  7.2 0.0 slice-done.3
  7.2 0.7 pad_maximum_fusion.refs_1_
  7.8 0.3 copy-done.1
  8.1 0.6 pad_slice_fusion
  8.8 141.5 %layer.1 = bf16[256,2048]{1,0:T(8,128)(2,1)} custom-call(bf16[256,2048]{1,0:T(8,128)(2,1)} %refs_0_.1, bf16[64,896]{1,0:T(8,128)(2,1)} %pad_maximum_fusion.refs_1_, bf16[64,512]{1,0:T(8,128)(2,1)} %pad_maximum_fusion.1.refs_2_, bf16[64,384]{1,0:T(8,128)(2,1)} %get-tuple-element.6.refs_3_, bf16[64,384]{1,0:T(8,128)(2,1)} %get-tuple-element.5.refs_4_, ...), custom_call_target="tpu_custom_call" | custom-call | tf_op jit(solution)/shard_map/layer/pallas_call | solution.py:468
  150.3 2.3 %copy.17 = bf16[256,2048]{1,0:T(8,128)(2,1)} copy(bf16[256,2048]{1,0:T(8,128)(2,1)} %layer.1) | data formatting | bytes 2097152
  (1 shorter events, 0.0 us)
Async XLA Ops:
  0.0 0.7 copy-start
  4.0 0.7 slice-start
  4.0 0.7 slice-start.2
  4.0 0.8 slice-start.4
  4.8 0.7 copy-start.2
  4.8 0.7 copy-start.3
  4.8 0.7 copy-start.4
  4.8 0.8 copy-start.5
  4.8 0.8 copy-start.6
  6.3 0.9 slice-start.1
  6.3 0.9 slice-start.3
  7.2 0.9 copy-start.1

commit v2 on v1

v2 whole, which is shorter than its diff:
```python
import functools
import heapq

import jax
import jax.numpy as jnp
from jax import lax
from jax.experimental import pallas as pl
from jax.experimental.pallas import tpu as pltpu
from jax.sharding import Mesh
from jax.sharding import PartitionSpec as P

DK = 64
DV = 128
FS = ("fs_0", "fs_1")
REP_FS = ("rep", "fs_0", "fs_1")
NZ, NY, NX = 8, 4, 4
ROWS = 256
D = 2048
SHARD = 64
COLS = 256
OWN = 32
LANES = 128

EPSILON = 1e-05
HEAD_FLOOR = 1.0
RESIDUAL_SCALE = 2.0**0.5
GATE_SOFTNESS = 16.0

MESH = pl.DeviceIdType.MESH
F32 = jnp.float32
BF16 = jnp.bfloat16
LINKS = ("z+", "z-", "y+", "y-")
WIDTHS = ((7, 4), (3, 3), (3, 1))
NEAREST = (0, 1, -1, 2, -2, 3, -3, 4)
CHUNK_LATE = (0.0, 3.33, 13.5)
FIRST_Z = (5.8, 6.9, 4.1, 3.2)
THEN_Y = (6.4, 0.0)
FIRST_Y = (8.4, 6.6)
THEN_Z = ((2.7, 6.6, 1.6, -2.6), (3.9, 1.4, 1.8, -1.1), (4.2, 1.6, 5.2, 1.5))
BACKLOG = 2.525


def gather_items():
    items = []

    def add(chunk, part, link, slot, half, rise):
        dz, dy = slot
        lands = {"z+": (dz - 1, dy), "z-": (dz + 1, dy), "y+": (dz, dy - 1), "y-": (dz, dy + 1)}[link]
        size = WIDTHS[chunk][part] * (1.0 if half is None else 0.5)
        items.append((chunk, part, link, slot, half, lands, CHUNK_LATE[chunk] - rise, size))

    def along_z(chunk, part, dy, rise):
        for s in range(4):
            add(chunk, part, "z+", (-s, dy), None if s < 3 else 0, rise[s])
            add(chunk, part, "z-", (s, dy), None if s < 3 else 1, rise[s])

    def along_y(chunk, part, dz, rise):
        add(chunk, part, "y+", (dz, 0), None, rise[0])
        add(chunk, part, "y-", (dz, 0), None, rise[0])
        add(chunk, part, "y+", (dz, -1), 0, rise[1])
        add(chunk, part, "y-", (dz, 1), 1, rise[1])

    for chunk in range(len(WIDTHS)):
        along_z(chunk, 0, 0, FIRST_Z)
        for dz in NEAREST:
            along_y(chunk, 0, dz, THEN_Y)
        along_y(chunk, 1, 0, FIRST_Y)
        for dy in (0, 1, -1, 2):
            along_z(chunk, 1, dy, THEN_Z[abs(dy)])
    return items


def spot(slot):
    return (slot[0] % NZ, slot[1] % NY)


def gather_order(backlog=BACKLOG, tile_us=0.352, fixed=0.05, hop=2.2):
    items = gather_items()
    held = {(c, p, (0, 0)): {0, 1} for c in range(len(WIDTHS)) for p in (0, 1)}
    waiting = list(range(len(items)))
    ready = {link: [] for link in LINKS}
    free = {link: 0.0 for link in LINKS}
    order, flying = [], []

    def step(now):
        left = []
        for i in waiting:
            chunk, part, link, slot, half = items[i][:5]
            have = held.get((chunk, part, spot(slot)), set())
            if have >= ({0, 1} if half is None else {half}):
                ready[link].append(i)
            else:
                left.append(i)
        waiting[:] = left
        for link in LINKS:
            ready[link].sort(key=lambda i: (items[i][6], i))
            while ready[link] and free[link] - now < backlog:
                i = ready[link].pop(0)
                free[link] = max(now, free[link]) + items[i][7] * tile_us + fixed
                heapq.heappush(flying, (free[link] + hop, i))
                order.append((now, "send", i))

    step(0.0)
    while flying:
        now, i = heapq.heappop(flying)
        chunk, part, _, _, half, lands = items[i][:6]
        held.setdefault((chunk, part, spot(lands)), set()).update({0, 1} if half is None else {half})
        order.append((now, "land", i))
        step(now)
    return items, order


def dot_nt(a, b):
    return lax.dot_general(a, b, (((1,), (1,)), ((), ())), preferred_element_type=F32)


def dot_nn(a, b, precision=None):
    return lax.dot_general(a, b, (((1,), (0,)), ((), ())), preferred_element_type=F32, precision=precision)


def silu(v):
    return v / (1.0 + jnp.exp(-v))


def boundary(prefix, m):
    if m >= 4:
        parts = prefix.reshape(ROWS // (2 * m), 2 * m, DK)
        edge = jnp.broadcast_to(parts[:, m - 1 : m, :], parts.shape)
        return edge.reshape(ROWS, DK)
    parts = prefix.reshape(ROWS // 8, 8, DK)
    row = lax.broadcasted_iota(jnp.int32, parts.shape, 1)
    edge = jnp.broadcast_to(parts[:, 8 - m - 1 : 8 - m, :], parts.shape)
    for at in range(8 - 4 * m, -1, -2 * m):
        edge = jnp.where(row < at + 2 * m, jnp.broadcast_to(parts[:, at + m - 1 : at + m, :], parts.shape), edge)
    return edge.reshape(ROWS, DK)


def head_out(q, k, v, log_decay):
    row = lax.broadcasted_iota(jnp.int32, (ROWS, ROWS), 0)
    col = lax.broadcasted_iota(jnp.int32, (ROWS, ROWS), 1)
    prefix = dot_nn((col <= row).astype(F32), log_decay, lax.Precision.HIGHEST)
    apart = row ^ col
    scores = jnp.where(row == col, jnp.sum(q * k, axis=1, keepdims=True), 0.0)
    m = ROWS // 2
    while m:
        fade = jnp.exp(-jnp.abs(prefix - boundary(prefix, m)))
        level = dot_nt((q * fade).astype(BF16), (k * fade).astype(BF16))
        scores = jnp.where((row > col) & (apart >= m) & (apart < 2 * m), level, scores)
        m //= 2
    return dot_nn(scores.astype(BF16), v.astype(BF16))


def layer_kernel(items, order, *refs):
    sources = refs[:15]
    out = refs[15]
    staged = refs[16:31]
    (tok, gate, up, down, query, key, value, outgate, output, rank_down, rank_up, bias, head_gain, norm_gain,
     norm_bias) = staged
    (GA, GB, DA, DB, QA, QB, acc, hid, first, second, third, mixed, sendbuf, pairbuf, xsend, xrecv, tot) = refs[31:48]
    (put_sem, get_sem, own_sem, pair_s, pair_r, x_s, x_r, ag_s, ag_r, out_sem) = refs[48:]
    bufs = ((GA, GB), (DA, DB), (QA, QB))
    cuts = [a * LANES for a, _ in WIDTHS]

    rep, zl, y, tp = (lax.axis_index(a) for a in ("rep", "fs_0", "fs_1", "tp"))
    zg = rep * NZ + zl
    x, c = tp // 2, lax.rem(tp, 2)
    other = 1 - c

    def at_z(step):
        g = lax.rem(zg + step + 16, 16)
        return (g // NZ, lax.rem(g, NZ), y, tp)

    def at_y(step):
        return (rep, zl, lax.rem(y + step + NY, NY), tp)

    def at_x(step):
        return (rep, zl, y, lax.rem(x + step + NX, NX) * 2 + c)

    partner = (rep, zl, y, x * 2 + other)
    where = {"z+": at_z(1), "z-": at_z(-1), "y+": at_y(1), "y-": at_y(-1)}
    xs = [at_x(s) for s in (1, 2, 3)]
    from_x = [lax.rem(x - s + NX, NX) for s in (1, 2, 3)]
    z_at = {k: lax.rem(zl + k, NZ) for k in range(NZ)}
    y_at = {k: lax.rem(y + k, NY) for k in range(NY)}

    barrier = pltpu.get_barrier_semaphore()
    friends = list(where.values()) + xs + [partner]
    for friend in friends:
        pl.semaphore_signal(barrier, inc=1, device_id=friend, device_id_type=MESH)
    loads = [pltpu.make_async_copy(a, b, own_sem.at[k]) for k, (a, b) in enumerate(zip(sources, staged))]
    for k in (1, 2, 3, 4, 5, 6, 7, 8, 0, 9, 10, 11, 12, 13, 14):
        loads[k].start()

    def pack(pair, cut, at, piece):
        stop = at + piece.shape[1]
        if at < cut:
            pair[0][zl, y, :, at : min(stop, cut)] = piece[:, : min(stop, cut) - at]
        if stop > cut:
            lo = max(at, cut)
            pair[1][zl, y, :, lo - cut : stop - cut] = piece[:, lo - at :]

    def side_by_side(a, b):
        return jnp.concatenate([a.astype(F32), b.astype(F32)], axis=1).astype(BF16)

    with jax.named_scope("pack"):
        for k in range(1, 9):
            loads[k].wait()
        pack(bufs[0], cuts[0], 0, gate[:, 0:640])
        pack(bufs[0], cuts[0], 640, up[:, 0:640])
        pack(bufs[0], cuts[0], 1280, side_by_side(gate[:, 640:704], up[:, 640:704]))
        pack(bufs[1], cuts[1], 0, down[:, 0:640])
        pack(bufs[1], cuts[1], 640, side_by_side(down[:, 640:704], jnp.zeros((SHARD, 64), BF16)))
        pack(bufs[2], cuts[2], 0, side_by_side(query[...], key[...]))
        pack(bufs[2], cuts[2], 128, value[...])
        pack(bufs[2], cuts[2], 256, outgate[...])
        pack(bufs[2], cuts[2], 384, output[...])
    with jax.named_scope("barrier"):
        pl.semaphore_wait(barrier, len(friends))

    def place(chunk, part, slot, half):
        dz, dy = spot(slot)
        buf = bufs[chunk][part]
        if half is None:
            return buf.at[z_at[dz], y_at[dy]]
        return buf.at[z_at[dz], y_at[dy], pl.ds(32 * half, 32)]

    def item_copy(i, landing):
        chunk, part, link, slot, half, lands = items[i][:6]
        here = place(chunk, part, lands if landing else slot, half)
        return pltpu.make_async_remote_copy(
            src_ref=here, dst_ref=here, send_sem=put_sem.at[i], recv_sem=get_sem.at[i],
            device_id=where[link], device_id_type=MESH)

    def near(i):
        return lax.rem(zl + ((i + 1) // 2) * (2 * lax.rem(i, 2) - 1) + NZ, NZ)

    def gate_up(source, rows, lo, hi):
        def step(i, carry):
            zi = near(i)
            a = source[:, pl.ds(pl.multiple_of(zi * COLS, COLS), COLS)]
            acc[rows, : cuts[0]] += dot_nn(a, GA[zi].reshape(COLS, cuts[0]))
            acc[rows, cuts[0] :] += dot_nn(a, GB[zi].reshape(COLS, 1408 - cuts[0]))
            return carry
        lax.fori_loop(lo, hi, step, 0)

    def clear(rows):
        acc[rows, :] = jnp.zeros((rows.stop - rows.start, 1408), F32)

    def hidden(rows):
        hid[rows, 0:640] = (silu(acc[rows, 0:640]) * acc[rows, 640:1280]).astype(BF16)
        last = acc[rows, 1280:1408]
        lane = lax.broadcasted_iota(jnp.int32, last.shape, 1)
        mixed_last = silu(last) * pltpu.roll(last, 64, 1)
        hid[rows, 640:768] = jnp.where(lane < 64, mixed_last, 0.0).astype(BF16)

    def down_part(rows):
        def part(zi):
            cut = cuts[1]
            return dot_nt(hid[rows, :cut], DA[zi].reshape(COLS, cut)) + dot_nt(
                hid[rows, cut:], DB[zi].reshape(COLS, 768 - cut))
        return part

    def pair_copy(zi, half):
        if half is None:
            src, dst, sem = sendbuf.at[zi, other], pairbuf.at[zi], 0
        else:
            rows, both = pl.ds(16 * half, 16), pl.ds(zi, 2)
            src, dst, sem = sendbuf.at[both, other, :, rows], pairbuf.at[both, :, rows], half
        return pltpu.make_async_remote_copy(
            src_ref=src, dst_ref=dst, send_sem=pair_s.at[sem, zi], recv_sem=pair_r.at[sem, zi],
            device_id=partner, device_id_type=MESH)

    def x_copy(zi, s, half):
        to = lax.rem(x + s + 1, NX)
        if half is None:
            src, dst, sem = xsend.at[zi, to], xrecv.at[s, zi], 0
        else:
            rows, both = pl.ds(16 * half, 16), pl.ds(zi, 2)
            src, dst, sem = xsend.at[both, to, rows], xrecv.at[s, both, rows], half
        return pltpu.make_async_remote_copy(
            src_ref=src, dst_ref=dst, send_sem=x_s.at[sem, s, zi], recv_sem=x_r.at[sem, s, zi],
            device_id=xs[s], device_id_type=MESH)

    def middle(zi, half):
        pair_copy(zi, half).wait_recv()
        if half is None:
            xsend[zi] = (sendbuf[zi, c].astype(F32) + pairbuf[zi].astype(F32)).astype(BF16)
        else:
            rows = slice(16 * half, 16 * half + 16)
            for k in range(2):
                xsend[zi + k, :, rows] = (
                    sendbuf[zi + k, c, :, rows].astype(F32) + pairbuf[zi + k, :, rows].astype(F32)
                ).astype(BF16)
        for s in (1, 0, 2):
            x_copy(zi, s, half).start()

    def settle(residual, store, factor, which, half):
        rows = slice(0, OWN) if half is None else slice(16 * half, 16 * half + 16)
        if half is None:
            def wait(zi, carry):
                for s in range(3):
                    x_copy(zi, s, None).wait_recv()
                return carry
            lax.fori_loop(0, NZ, wait, 0)
        else:
            def wait(k, carry):
                for s in range(3):
                    x_copy(2 * k, s, half).wait_recv()
                return carry
            lax.fori_loop(0, NZ // 2, wait, 0)
        own = residual.astype(F32)
        total = 0.0
        for zi in range(NZ):
            part = sendbuf[zi, c, x, rows].astype(F32) + pairbuf[zi, x, rows].astype(F32)
            for s in range(3):
                part = part + xrecv[s, zi, rows].astype(F32)
            part = RESIDUAL_SCALE * own[:, zi * COLS : (zi + 1) * COLS] + factor * part
            tot[rows, zi * COLS : (zi + 1) * COLS] = part
            total = total + jnp.sum(part, axis=1, keepdims=True)
        centred = tot[rows, :] - total * (1.0 / D)
        spread = jnp.mean(centred * centred, axis=1, keepdims=True)
        normed = centred * lax.rsqrt(spread + EPSILON) * norm_gain[which : which + 1, :] + norm_bias[which : which + 1, :]
        store(normed.astype(BF16))

    def block(target, xx, cc, half):
        t = xx * 2 + cc
        if target is second:
            return target.at[half, pl.ds(pl.multiple_of(t * 16, 16), 16)]
        return target.at[pl.ds(pl.multiple_of(t * OWN + 16 * half, 16), 16)]

    def ag_copy(target, k, half, xx, cc, to):
        ref = block(target, xx, cc, half)
        return pltpu.make_async_remote_copy(
            src_ref=ref, dst_ref=ref, send_sem=ag_s.at[k, half], recv_sem=ag_r.at[k, half],
            device_id=to, device_id_type=MESH)

    def spread_out(target, half):
        for s in (1, 0, 2):
            ag_copy(target, s, half, x, c, xs[s]).start()
        ag_copy(target, 3, half, x, c, partner).start()

    def pass_on(target, s, half):
        ag_copy(target, s, half, from_x[s], c, xs[s]).wait_recv()
        ag_copy(target, 4 + s, half, from_x[s], c, partner).start()

    def pass_all(target, half):
        for s in (0, 2, 1):
            pass_on(target, s, half)

    def gathered(target, half):
        ag_copy(target, 3, half, x, other, partner).wait_recv()
        for s in range(3):
            ag_copy(target, 4 + s, half, from_x[s], other, partner).wait_recv()

    def drain_rows(target, half):
        for s in range(3):
            ag_copy(target, s, half, x, c, xs[s]).wait_send()
            ag_copy(target, 4 + s, half, from_x[s], c, partner).wait_send()
        ag_copy(target, 3, half, x, c, partner).wait_send()

    def drain_sums(half):
        stride = 1 if half is None else 2

        def wait(k, carry):
            pair_copy(k * stride, half).wait_send()
            for s in range(3):
                x_copy(k * stride, s, half).wait_send()
            return carry
        lax.fori_loop(0, NZ // stride, wait, 0)

    every = slice(0, ROWS)
    row0 = pl.multiple_of(tp * OWN, OWN)
    held = {}
    done_groups = [[], [], []]
    state = {"gate": 0, "fronts": [], "middles": []}
    end_of = [max(t for t, kind, i in order if kind == "land" and items[i][0] == k) for k in range(3)]
    steps = [(t, 0, kind, i) for t, kind, i in order]
    steps += [(end_of[1] + 4.5, 1, "settle", 0)]
    at = end_of[1] + 8.0
    for half in range(2):
        for s in (0, 2, 1):
            steps.append((at + 1.5 * half + (0.7 if s == 1 else 0.0), 3, "pass", (s, half)))
    steps.sort(key=lambda e: e[:2])
    clear(every)
    loads[0].wait()
    for k in range(9, 15):
        loads[k].wait()

    def first_front(zi):
        value = down_part(every)(zi)
        for t in range(8):
            sendbuf[zi, t % 2, t // 2] = value[t * OWN : (t + 1) * OWN].astype(BF16)
        pair_copy(zi, None).start()

    def flush_middles(keep):
        while len(state["middles"]) > keep:
            with jax.named_scope("mid1"):
                middle(state["middles"].pop(0), None)

    for now, _, kind, what in steps:
        if kind == "send":
            item_copy(what, False).start()
        elif kind == "land":
            chunk, part, _, _, half, lands = items[what][:6]
            with jax.named_scope("land%d" % chunk):
                item_copy(what, True).wait_recv()
            key_ = (chunk, spot(lands)[0])
            held[key_] = held.get(key_, 0.0) + (1.0 if half is None else 0.5)
            full = 6.0 if spot(lands)[0] == 0 else 8.0
            if held[key_] == full:
                done_groups[chunk].append(spot(lands)[0])
            if chunk == 0 and {spot((k, 0))[0] for k in NEAREST[:5]} <= set(done_groups[0]) and state["gate"] == 0:
                with jax.named_scope("gu_a"):
                    gate_up(tok, every, 0, 5)
                state["gate"] = 5
            if chunk == 0 and len(done_groups[0]) == NZ and state["gate"] == 5:
                with jax.named_scope("gu_b"):
                    gate_up(tok, every, 5, 8)
                    hidden(every)
                state["gate"] = 8
            if state["gate"] == 8:
                for k in done_groups[1]:
                    if k not in state["fronts"]:
                        state["fronts"].append(k)
                        with jax.named_scope("front1"):
                            first_front(z_at[k])
                        state["middles"].append(z_at[k])
                        flush_middles(2)
                if len(state["fronts"]) == NZ:
                    flush_middles(0)
        elif kind == "settle":
            def store_first(normed):
                first[pl.ds(row0, OWN), :] = normed
            with jax.named_scope("settle1"):
                settle(tok[pl.ds(row0, OWN), :], store_first, 0.5, 0, None)
            spread_out(first, 0)
            spread_out(first, 1)
        else:
            with jax.named_scope("pass1"):
                pass_on(first, *what)
    with jax.named_scope("gathered1"):
        gathered(first, 0)
        gathered(first, 1)

    with jax.named_scope("proj"):
        rows = first[...]
        pieces = [dot_nn(rows, QA[...].reshape(D, cuts[2]))]
        if cuts[2] < 384:
            pieces.append(dot_nn(rows, QB[:, :, :, : 384 - cuts[2]].reshape(D, 384 - cuts[2])))
        proj = jnp.concatenate(pieces, axis=1)
        ranks = dot_nt(rows, rank_down[...])
        pair_at = pl.multiple_of(x * 128, 128)

        def mine(ref):
            both = ref[:, pl.ds(pair_at, 128)].astype(F32)
            return jnp.where(c == 0, both[:, :64], both[:, 64:])
        source = dot_nn(ranks, mine(rank_up), lax.Precision.HIGHEST) + mine(bias)
        log_decay = (jnp.minimum(source, 0.0) - jnp.log1p(jnp.exp(-jnp.abs(source)))) * (1.0 / GATE_SOFTNESS)
    with jax.named_scope("gla"):
        heads = head_out(proj[:, :DK] * DK**-0.5, proj[:, DK : 2 * DK], proj[:, 128:256], log_decay)
        scale = lax.rsqrt(jnp.mean(heads * heads, axis=1, keepdims=True) + HEAD_FLOOR)
        gain = head_gain[:, pl.ds(pl.multiple_of(tp * DV, DV), DV)]
        mixed[...] = (heads * scale * gain * silu(proj[:, 256:384])).astype(BF16)
    drain_sums(None)

    def output_fronts(k):
        part = dot_nt(mixed[...], QB[4 * k : 4 * k + 4, :, :, -128:].reshape(4 * COLS, 128))
        for g in range(4):
            for t in range(8):
                sendbuf[4 * k + g, t % 2, t // 2] = part[
                    t * OWN : (t + 1) * OWN, g * COLS : (g + 1) * COLS].astype(BF16)
        for half in range(2):
            for g in range(0, 4, 2):
                pair_copy(4 * k + g, half).start()

    def middles(half, lo, hi):
        def step(k, carry):
            middle(2 * k, half)
            return carry
        lax.fori_loop(lo, hi, step, 0)

    with jax.named_scope("rs2"):
        output_fronts(0)
        output_fronts(1)
        middles(0, 0, 4)
        middles(1, 0, 4)

    leaving = []

    def put_out(k, half, xx, cc):
        copy = pltpu.make_async_copy(block(third, xx, cc, half), block(out, xx, cc, half), out_sem.at[k, half])
        copy.start()
        leaving.append(copy)

    def settle_second(half):
        def store(normed):
            second[half, pl.ds(pl.multiple_of(tp * 16, 16), 16), :] = normed
        start = pl.multiple_of(row0 + 16 * half, 16)
        settle(first[pl.ds(start, 16), :], store, 1.0, 1, half)
        spread_out(second, half)

    def settle_last(half):
        def store(normed):
            third[pl.ds(pl.multiple_of(row0 + 16 * half, 16), 16), :] = normed
        settle(second[half, pl.ds(pl.multiple_of(tp * 16, 16), 16), :], store, 0.5, 2, half)
        spread_out(third, half)
        put_out(7, half, x, c)

    def rows_of(half):
        return slice(128 * half, 128 * half + 128)

    def mixer_front(half):
        rows = rows_of(half)
        acc[rows, : cuts[0]] = dot_nn(second[half], GA[...].reshape(D, cuts[0]))
        acc[rows, cuts[0] :] = dot_nn(second[half], GB[...].reshape(D, 1408 - cuts[0]))
        hidden(rows)

    def down_sums(half):
        rows, cut = rows_of(half), cuts[1]
        for k in range(2):
            groups = slice(4 * k, 4 * k + 4)
            part = dot_nt(hid[rows, :cut], DA[groups].reshape(4 * COLS, cut)) + dot_nt(
                hid[rows, cut:], DB[groups].reshape(4 * COLS, 768 - cut))
            for g in range(4):
                for t in range(8):
                    sendbuf[4 * k + g, t % 2, t // 2, 16 * half : 16 * half + 16] = part[
                        t * 16 : (t + 1) * 16, g * COLS : (g + 1) * COLS].astype(BF16)
            for g in range(0, 4, 2):
                pair_copy(4 * k + g, half).start()
        middles(half, 0, 4)

    with jax.named_scope("settle2a"):
        settle_second(0)
    with jax.named_scope("settle2b"):
        settle_second(1)
    with jax.named_scope("pass2a"):
        pass_all(second, 0)
        gathered(second, 0)
    with jax.named_scope("gu2a"):
        mixer_front(0)
    with jax.named_scope("pass2b"):
        pass_all(second, 1)
    with jax.named_scope("rs3a"):
        drain_sums(0)
        down_sums(0)
    with jax.named_scope("gathered2b"):
        gathered(second, 1)
    with jax.named_scope("gu2b"):
        mixer_front(1)
    with jax.named_scope("rs3b"):
        drain_sums(1)
        down_sums(1)
    for half in range(2):
        drain_rows(first, half)
        drain_rows(second, half)
    with jax.named_scope("settle3a"):
        settle_last(0)
    with jax.named_scope("settle3b"):
        settle_last(1)
    for half in range(2):
        with jax.named_scope("pass3"):
            for s in (0, 2, 1):
                pass_on(third, s, half)
                put_out(s, half, from_x[s], c)
    with jax.named_scope("puts"):
        for _, kind, i in order:
            if kind == "send":
                item_copy(i, False).wait_send()
    for half in range(2):
        with jax.named_scope("gathered3"):
            ag_copy(third, 3, half, x, other, partner).wait_recv()
            put_out(3, half, x, other)
            for s in (0, 2, 1):
                ag_copy(third, 4 + s, half, from_x[s], other, partner).wait_recv()
                put_out(4 + s, half, from_x[s], other)
    with jax.named_scope("drain"):
        for half in range(2):
            drain_sums(half)
            drain_rows(third, half)
        for copy in leaving:
            copy.wait()


def per_device(
    tokens, ffn_gate, ffn_up, ffn_down, query_proj, key_proj, value_proj, outgate_proj, output_proj,
    rank_down, rank_up, decay_bias, head_gain, norm_gain, norm_bias,
):
    operands = (
        tokens, ffn_gate, ffn_up, ffn_down.T, query_proj, key_proj, value_proj, outgate_proj, output_proj.T,
        rank_down.T, rank_up, decay_bias.reshape(1, -1), head_gain.reshape(1, -1), norm_gain, norm_bias,
    )
    items, order = gather_order()
    count = len(items)
    dma = pltpu.SemaphoreType.DMA
    scratch = [pltpu.VMEM(a.shape, a.dtype) for a in operands]
    scratch += [pltpu.VMEM((NZ, NY, SHARD, tiles * LANES), BF16) for pair in WIDTHS for tiles in pair]
    scratch += [
        pltpu.VMEM((ROWS, 1408), F32),
        pltpu.VMEM((ROWS, 768), BF16),
        pltpu.VMEM((ROWS, D), BF16),
        pltpu.VMEM((2, ROWS // 2, D), BF16),
        pltpu.VMEM((ROWS, D), BF16),
        pltpu.VMEM((ROWS, DV), BF16),
        pltpu.VMEM((NZ, 2, NX, OWN, COLS), BF16),
        pltpu.VMEM((NZ, NX, OWN, COLS), BF16),
        pltpu.VMEM((NZ, NX, OWN, COLS), BF16),
        pltpu.VMEM((3, NZ, OWN, COLS), BF16),
        pltpu.VMEM((OWN, D), F32),
        dma((count,)), dma((count,)), dma((15,)),
        dma((2, NZ)), dma((2, NZ)), dma((2, 3, NZ)), dma((2, 3, NZ)), dma((7, 2)), dma((7, 2)), dma((8, 2)),
    ]
    rows = pl.pallas_call(
        functools.partial(layer_kernel, items, order),
        out_shape=jax.ShapeDtypeStruct((ROWS, D), BF16),
        in_specs=[pl.BlockSpec(memory_space=pltpu.HBM)] * 15,
        out_specs=pl.BlockSpec(memory_space=pltpu.HBM),
        scratch_shapes=scratch,
        compiler_params=pltpu.CompilerParams(
            collective_id=0, has_side_effects=True, vmem_limit_bytes=60 * 1024 * 1024),
        name="layer",
    )(*operands)
    return jnp.where(lax.axis_index("tp") >= 0, rows, jnp.zeros_like(rows))


def solution(mesh):
    finer = Mesh(
        mesh.devices.reshape(mesh.shape["rep"], NZ, NY, mesh.shape["tp"]),
        ("rep", "fs_0", "fs_1", "tp"),
    )
    return jax.shard_map(
        per_device,
        mesh=finer,
        in_specs=(
            P(REP_FS, None), P(FS, "tp"), P(FS, "tp"), P("tp", FS), P(FS, "tp"), P(FS, "tp"), P(FS, "tp"),
            P(FS, "tp"), P("tp", FS), P(), P(), P(), P(), P(), P(),
        ),
        out_specs=P(REP_FS, None),
        check_vma=False,
    )
```

time: 153 us -> 128 us (0.84)
  Pallas kernels: 142 us -> 125 us
  local copies, waits for them, and re-layouts: 7.62 us -> 0 us
    pallas_call x1, Pallas kernels: 142 us -> 125 us  [per_device(): pl.pallas_call(functools.partial(layer_kernel, items, order), out_shape=j...]
    unnamed x15 -> x0, local copies, waits for them, and re-layouts: 3.32 us -> none
    slice x11 -> x0, local copies, waits for them, and re-layouts: 2.36 us -> none  [the longest x4 0.89 us: per_device(): ga = jnp.concatenate([ffn_gate[:, :640], ffn_up[:, :256]], axis=1)]
    select_n x0 -> x1, other arithmetic: none -> 2.27 us  [per_device(): return jnp.where(lax.axis_index('tp') >= 0, rows, jnp.zeros_like(rows))]
    concatenate x3 -> x0, other arithmetic: 2.07 us -> none  [the longest x1 0.71 us: per_device(): jnp.concatenate([ffn_up[:, 256:640], ffn_gate[:, 640:], ffn_up[:, 640:]],...]
    reshape x2 -> x0, local copies, waits for them, and re-layouts: 1.93 us -> none  [the longest x1 1.29 us: per_device(): lax.dynamic_slice_in_dim(decay_bias, tp * DK, DK, 0).reshape(1, DK)]
where the time goes in v2:
time: 128 us; the launch traced here: 127 us
  Pallas kernels  125 us (98%)
  other arithmetic  2.27 us (2%)
    pallas_call x1, Pallas kernels, per_device(): pl.pallas_call(functools.partial(layer_kernel, items, order), out_shape=j...  125 us

profile of v2, /device:TPU:1, one launch (start us, length us, event | category | flops | bytes accessed | tf_op | source)
XLA Modules:
  0.0 127.4 jit_solution(11205375149530438982)
XLA Ops:
  0.0 125.1 %layer.1 = bf16[256,2048]{1,0:T(8,128)(2,1)} custom-call(bf16[256,2048]{1,0:T(8,128)(2,1)} %refs_0_.1, bf16[64,704]{1,0:T(8,128)(2,1)} %refs_1_.1, bf16[64,704]{1,0:T(8,128)(2,1)} %refs_2_.1, bf16[64,704]{1,0:T(8,128)(2,1)} %bitcast.5, bf16[64,64]{1,0:T(8,128)(2,1)} %refs_4_.1, bf16[64,64]{1,0:T(8,128)(2,1)} %refs_5_.1, bf16[64,128]{1,0:T(8,128)(2,1)} %refs_6_.1, ...), custom_call_target="tpu_custom_call" | custom-call | tf_op jit(solution)/shard_map/layer/pallas_call | solution.py:612
  125.1 2.3 %broadcast_select_fusion = bf16[256,2048]{1,0:T(8,128)(2,1)} fusion(bf16[256,2048]{1,0:T(8,128)(2,1)} %layer.1, pred[]{:T(512)S(6)} %ge.3), kind=kLoop, calls=%fused_computation | loop fusion | flops 524288 | bytes 2097153 | tf_op jit(solution)/shard_map/jit(_where)/select_n | solution.py:622

commit v3 on v2

--- a/solution.py
+++ b/solution.py
@@ -38,27 +38,36 @@
 FIRST_Y = (8.4, 6.6)
 THEN_Z = ((2.7, 6.6, 1.6, -2.6), (3.9, 1.4, 1.8, -1.1), (4.2, 1.6, 5.2, 1.5))
 BACKLOG = 2.525
+MIDDLES_AT = ((-2.0, 1), (-1.0, 1), (0.0, 1), (1.5, 0))
+SETTLE_AT = 4.5
+PASS_AT = 11.0
+
+
+def spot(slot):
+    return (slot[0] % NZ, slot[1] % NY)
 
 
 def gather_items():
-    items = []
-
-    def add(chunk, part, link, slot, half, rise):
-        dz, dy = slot
-        lands = {"z+": (dz - 1, dy), "z-": (dz + 1, dy), "y+": (dz, dy - 1), "y-": (dz, dy + 1)}[link]
-        size = WIDTHS[chunk][part] * (1.0 if half is None else 0.5)
-        items.append((chunk, part, link, slot, half, lands, CHUNK_LATE[chunk] - rise, size))
+    items, groups = [], []
+
+    def add(chunk, part, pair, rise):
+        members = []
+        for link, slot, half in pair:
+            dz, dy = slot
+            lands = {"z+": (dz - 1, dy), "z-": (dz + 1, dy), "y+": (dz, dy - 1), "y-": (dz, dy + 1)}[link]
+            size = WIDTHS[chunk][part] * (1.0 if half is None else 0.5)
+            members.append(len(items))
+            items.append((chunk, part, link, slot, half, lands, CHUNK_LATE[chunk] - rise, size, len(groups)))
+        groups.append(members)
 
     def along_z(chunk, part, dy, rise):
         for s in range(4):
-            add(chunk, part, "z+", (-s, dy), None if s < 3 else 0, rise[s])
-            add(chunk, part, "z-", (s, dy), None if s < 3 else 1, rise[s])
+            halves = (None, None) if s < 3 else (0, 1)
+            add(chunk, part, [("z+", (-s, dy), halves[0]), ("z-", (s, dy), halves[1])], rise[s])
 
     def along_y(chunk, part, dz, rise):
-        add(chunk, part, "y+", (dz, 0), None, rise[0])
-        add(chunk, part, "y-", (dz, 0), None, rise[0])
-        add(chunk, part, "y+", (dz, -1), 0, rise[1])
-        add(chunk, part, "y-", (dz, 1), 1, rise[1])
+        add(chunk, part, [("y+", (dz, 0), None), ("y-", (dz, 0), None)], rise[0])
+        add(chunk, part, [("y+", (dz, -1), 0), ("y-", (dz, 1), 1)], rise[1])
 
     for chunk in range(len(WIDTHS)):
         along_z(chunk, 0, 0, FIRST_Z)
@@ -67,17 +76,14 @@
         along_y(chunk, 1, 0, FIRST_Y)
         for dy in (0, 1, -1, 2):
             along_z(chunk, 1, dy, THEN_Z[abs(dy)])
-    return items
-
-
-def spot(slot):
-    return (slot[0] % NZ, slot[1] % NY)
-
-
-def gather_order(backlog=BACKLOG, tile_us=0.352, fixed=0.05, hop=2.2):
-    items = gather_items()
+    return items, groups
+
+
+def gather_order(tile_us=0.352, fixed=0.05, hop=2.9):
+    items, groups = gather_items()
     held = {(c, p, (0, 0)): {0, 1} for c in range(len(WIDTHS)) for p in (0, 1)}
     waiting = list(range(len(items)))
+    missing = [len(members) for members in groups]
     ready = {link: [] for link in LINKS}
     free = {link: 0.0 for link in LINKS}
     order, flying = [], []
@@ -88,14 +94,13 @@
             chunk, part, link, slot, half = items[i][:5]
             have = held.get((chunk, part, spot(slot)), set())
             if have >= ({0, 1} if half is None else {half}):
-                ready[link].append(i)
+                heapq.heappush(ready[link], (items[i][6], i))
             else:
                 left.append(i)
         waiting[:] = left
         for link in LINKS:
-            ready[link].sort(key=lambda i: (items[i][6], i))
-            while ready[link] and free[link] - now < backlog:
-                i = ready[link].pop(0)
+            while ready[link] and free[link] - now < BACKLOG:
+                _, i = heapq.heappop(ready[link])
                 free[link] = max(now, free[link]) + items[i][7] * tile_us + fixed
                 heapq.heappush(flying, (free[link] + hop, i))
                 order.append((now, "send", i))
@@ -103,11 +108,16 @@
     step(0.0)
     while flying:
         now, i = heapq.heappop(flying)
-        chunk, part, _, _, half, lands = items[i][:6]
-        held.setdefault((chunk, part, spot(lands)), set()).update({0, 1} if half is None else {half})
-        order.append((now, "land", i))
+        group = items[i][8]
+        missing[group] -= 1
+        if missing[group]:
+            continue
+        for k in groups[group]:
+            chunk, part, _, _, half, lands = items[k][:6]
+            held.setdefault((chunk, part, spot(lands)), set()).update({0, 1} if half is None else {half})
+        order.append((now, "land", group))
         step(now)
-    return items, order
+    return items, groups, order
 
 
 def dot_nt(a, b):
@@ -150,14 +160,14 @@
     return dot_nn(scores.astype(BF16), v.astype(BF16))
 
 
-def layer_kernel(items, order, *refs):
+def layer_kernel(items, groups, order, *refs):
     sources = refs[:15]
     out = refs[15]
     staged = refs[16:31]
     (tok, gate, up, down, query, key, value, outgate, output, rank_down, rank_up, bias, head_gain, norm_gain,
      norm_bias) = staged
-    (GA, GB, DA, DB, QA, QB, acc, hid, first, second, third, mixed, sendbuf, pairbuf, xsend, xrecv, tot) = refs[31:48]
-    (put_sem, get_sem, own_sem, pair_s, pair_r, x_s, x_r, ag_s, ag_r, out_sem) = refs[48:]
+    (GA, GB, DA, DB, QA, QB, acc, hid, first, second, third, mixed, projected, sendbuf, pairbuf, xsend, xrecv, tot) = refs[31:49]
+    (put_sem, get_sem, own_sem, pair_s, pair_r, x_s, x_r, ag_s, ag_r, out_sem) = refs[49:]
     bufs = ((GA, GB), (DA, DB), (QA, QB))
     cuts = [a * LANES for a, _ in WIDTHS]
 
@@ -191,13 +201,15 @@
     for k in (1, 2, 3, 4, 5, 6, 7, 8, 0, 9, 10, 11, 12, 13, 14):
         loads[k].start()
 
+    mine_at = zl * NY + y
+
     def pack(pair, cut, at, piece):
         stop = at + piece.shape[1]
         if at < cut:
-            pair[0][zl, y, :, at : min(stop, cut)] = piece[:, : min(stop, cut) - at]
+            pair[0][mine_at, :, at : min(stop, cut)] = piece[:, : min(stop, cut) - at]
         if stop > cut:
             lo = max(at, cut)
-            pair[1][zl, y, :, lo - cut : stop - cut] = piece[:, lo - at :]
+            pair[1][mine_at, :, lo - cut : stop - cut] = piece[:, lo - at :]
 
     def side_by_side(a, b):
         return jnp.concatenate([a.astype(F32), b.astype(F32)], axis=1).astype(BF16)
@@ -219,29 +231,40 @@
 
     def place(chunk, part, slot, half):
         dz, dy = spot(slot)
-        buf = bufs[chunk][part]
+        at = z_at[dz] * NY + y_at[dy]
         if half is None:
-            return buf.at[z_at[dz], y_at[dy]]
-        return buf.at[z_at[dz], y_at[dy], pl.ds(32 * half, 32)]
-
-    def item_copy(i, landing):
-        chunk, part, link, slot, half, lands = items[i][:6]
-        here = place(chunk, part, lands if landing else slot, half)
+            return bufs[chunk][part].at[at]
+        return bufs[chunk][part].at[at, pl.ds(32 * half, 32)]
+
+    def put(i):
+        chunk, part, link, slot, half = items[i][:5]
+        here = place(chunk, part, slot, half)
+        pltpu.make_async_remote_copy(
+            src_ref=here, dst_ref=here, send_sem=put_sem.at[2 * chunk + part], recv_sem=get_sem.at[items[i][8]],
+            device_id=where[link], device_id_type=MESH).start()
+
+    def bytes_of(chunk, part, slabs, group):
+        count = bufs[chunk][part].at[pl.ds(0, slabs)]
         return pltpu.make_async_remote_copy(
-            src_ref=here, dst_ref=here, send_sem=put_sem.at[i], recv_sem=get_sem.at[i],
-            device_id=where[link], device_id_type=MESH)
-
-    def near(i):
-        return lax.rem(zl + ((i + 1) // 2) * (2 * lax.rem(i, 2) - 1) + NZ, NZ)
-
-    def gate_up(source, rows, lo, hi):
-        def step(i, carry):
-            zi = near(i)
-            a = source[:, pl.ds(pl.multiple_of(zi * COLS, COLS), COLS)]
-            acc[rows, : cuts[0]] += dot_nn(a, GA[zi].reshape(COLS, cuts[0]))
-            acc[rows, cuts[0] :] += dot_nn(a, GB[zi].reshape(COLS, 1408 - cuts[0]))
-            return carry
-        lax.fori_loop(lo, hi, step, 0)
+            src_ref=count, dst_ref=count, send_sem=put_sem.at[2 * chunk + part], recv_sem=get_sem.at[group],
+            device_id=where["z+"], device_id_type=MESH)
+
+    def landed(group):
+        chunk, part, _, _, half = items[groups[group][0]][:5]
+        bytes_of(chunk, part, 2 if half is None else 1, group).wait_recv()
+
+    def all_put():
+        for chunk in range(len(WIDTHS)):
+            for part in range(2):
+                bytes_of(chunk, part, NZ * NY - 1, 0).wait_send()
+
+    def group_of(buf, zi, count=1):
+        return buf[pl.ds(zi * NY, NY * count)].reshape(COLS * count, buf.shape[2])
+
+    def gate_up(zi):
+        a = tok[:, pl.ds(pl.multiple_of(zi * COLS, COLS), COLS)]
+        acc[:, : cuts[0]] += dot_nn(a, group_of(GA, zi))
+        acc[:, cuts[0] :] += dot_nn(a, group_of(GB, zi))
 
     def clear(rows):
         acc[rows, :] = jnp.zeros((rows.stop - rows.start, 1408), F32)
@@ -256,18 +279,17 @@
     def down_part(rows):
         def part(zi):
             cut = cuts[1]
-            return dot_nt(hid[rows, :cut], DA[zi].reshape(COLS, cut)) + dot_nt(
-                hid[rows, cut:], DB[zi].reshape(COLS, 768 - cut))
+            return dot_nt(hid[rows, :cut], group_of(DA, zi)) + dot_nt(hid[rows, cut:], group_of(DB, zi))
         return part
 
     def pair_copy(zi, half):
         if half is None:
-            src, dst, sem = sendbuf.at[zi, other], pairbuf.at[zi], 0
+            src, dst, sem, out_of = sendbuf.at[zi, other], pairbuf.at[zi], zi, 0
         else:
             rows, both = pl.ds(16 * half, 16), pl.ds(zi, 2)
-            src, dst, sem = sendbuf.at[both, other, :, rows], pairbuf.at[both, :, rows], half
+            src, dst, sem, out_of = sendbuf.at[both, other, :, rows], pairbuf.at[both, :, rows], 4 * half + zi // 2, half
         return pltpu.make_async_remote_copy(
-            src_ref=src, dst_ref=dst, send_sem=pair_s.at[sem, zi], recv_sem=pair_r.at[sem, zi],
+            src_ref=src, dst_ref=dst, send_sem=pair_s.at[out_of], recv_sem=pair_r.at[sem],
             device_id=partner, device_id_type=MESH)
 
     def x_copy(zi, s, half):
@@ -278,7 +300,15 @@
             rows, both = pl.ds(16 * half, 16), pl.ds(zi, 2)
             src, dst, sem = xsend.at[both, to, rows], xrecv.at[s, both, rows], half
         return pltpu.make_async_remote_copy(
-            src_ref=src, dst_ref=dst, send_sem=x_s.at[sem, s, zi], recv_sem=x_r.at[sem, s, zi],
+            src_ref=src, dst_ref=dst, send_sem=x_s.at[sem, s], recv_sem=x_r.at[sem, s],
+            device_id=xs[s], device_id_type=MESH)
+
+    def sums_of(half, s):
+        rows = pl.ds(0, OWN) if half is None else pl.ds(16 * half, 16)
+        sem = 0 if half is None else half
+        ref = xrecv.at[s, :, rows]
+        return pltpu.make_async_remote_copy(
+            src_ref=ref, dst_ref=ref, send_sem=x_s.at[sem, s], recv_sem=x_r.at[sem, s],
             device_id=xs[s], device_id_type=MESH)
 
     def middle(zi, half):
@@ -296,18 +326,8 @@
 
     def settle(residual, store, factor, which, half):
         rows = slice(0, OWN) if half is None else slice(16 * half, 16 * half + 16)
-        if half is None:
-            def wait(zi, carry):
-                for s in range(3):
-                    x_copy(zi, s, None).wait_recv()
-                return carry
-            lax.fori_loop(0, NZ, wait, 0)
-        else:
-            def wait(k, carry):
-                for s in range(3):
-                    x_copy(2 * k, s, half).wait_recv()
-                return carry
-            lax.fori_loop(0, NZ // 2, wait, 0)
+        for s in range(3):
+            sums_of(half, s).wait_recv()
         own = residual.astype(F32)
         total = 0.0
         for zi in range(NZ):
@@ -324,14 +344,14 @@
 
     def block(target, xx, cc, half):
         t = xx * 2 + cc
-        if target is second:
+        if target is not third and target is not out:
             return target.at[half, pl.ds(pl.multiple_of(t * 16, 16), 16)]
         return target.at[pl.ds(pl.multiple_of(t * OWN + 16 * half, 16), 16)]
 
     def ag_copy(target, k, half, xx, cc, to):
         ref = block(target, xx, cc, half)
         return pltpu.make_async_remote_copy(
-            src_ref=ref, dst_ref=ref, send_sem=ag_s.at[k, half], recv_sem=ag_r.at[k, half],
+            src_ref=ref, dst_ref=ref, send_sem=ag_s.at[half], recv_sem=ag_r.at[k, half],
             device_id=to, device_id_type=MESH)
 
     def spread_out(target, half):
@@ -352,34 +372,31 @@
         for s in range(3):
             ag_copy(target, 4 + s, half, from_x[s], other, partner).wait_recv()
 
-    def drain_rows(target, half):
+    def drain_rows(half):
+        ref = second.at[0, pl.ds(0, 112)]
+        pltpu.make_async_remote_copy(
+            src_ref=ref, dst_ref=ref, send_sem=ag_s.at[half], recv_sem=ag_r.at[0, half],
+            device_id=partner, device_id_type=MESH).wait_send()
+
+    def drain_sums(half):
+        rows = pl.ds(0, OWN) if half is None else pl.ds(16 * half, 16)
+        ref = pairbuf.at[:, :, rows]
+        pltpu.make_async_remote_copy(
+            src_ref=ref, dst_ref=ref, send_sem=pair_s.at[0 if half is None else half], recv_sem=pair_r.at[0],
+            device_id=partner, device_id_type=MESH).wait_send()
         for s in range(3):
-            ag_copy(target, s, half, x, c, xs[s]).wait_send()
-            ag_copy(target, 4 + s, half, from_x[s], c, partner).wait_send()
-        ag_copy(target, 3, half, x, c, partner).wait_send()
-
-    def drain_sums(half):
-        stride = 1 if half is None else 2
-
-        def wait(k, carry):
-            pair_copy(k * stride, half).wait_send()
-            for s in range(3):
-                x_copy(k * stride, s, half).wait_send()
-            return carry
-        lax.fori_loop(0, NZ // stride, wait, 0)
+            sums_of(half, s).wait_send()
 
     every = slice(0, ROWS)
     row0 = pl.multiple_of(tp * OWN, OWN)
     held = {}
     done_groups = [[], [], []]
     state = {"gate": 0, "fronts": [], "middles": []}
-    end_of = [max(t for t, kind, i in order if kind == "land" and items[i][0] == k) for k in range(3)]
+    end_of = [max(t for t, kind, g in order if kind == "land" and items[groups[g][0]][0] == k) for k in range(3)]
     steps = [(t, 0, kind, i) for t, kind, i in order]
-    steps += [(end_of[1] + 4.5, 1, "settle", 0)]
-    at = end_of[1] + 8.0
-    for half in range(2):
-        for s in (0, 2, 1):
-            steps.append((at + 1.5 * half + (0.7 if s == 1 else 0.0), 3, "pass", (s, half)))
+    steps += [(end_of[1] + at, 1, "middles", keep) for at, keep in MIDDLES_AT]
+    steps += [(end_of[1] + SETTLE_AT, 2, "settle", 0)]
+    steps += [(end_of[1] + PASS_AT + 2.5 * half, 3, "pass", half) for half in range(2)]
     steps.sort(key=lambda e: e[:2])
     clear(every)
     loads[0].wait()
@@ -399,56 +416,62 @@
 
     for now, _, kind, what in steps:
         if kind == "send":
-            item_copy(what, False).start()
+            put(what)
         elif kind == "land":
-            chunk, part, _, _, half, lands = items[what][:6]
+            chunk = items[groups[what][0]][0]
             with jax.named_scope("land%d" % chunk):
-                item_copy(what, True).wait_recv()
-            key_ = (chunk, spot(lands)[0])
-            held[key_] = held.get(key_, 0.0) + (1.0 if half is None else 0.5)
-            full = 6.0 if spot(lands)[0] == 0 else 8.0
-            if held[key_] == full:
-                done_groups[chunk].append(spot(lands)[0])
-            if chunk == 0 and {spot((k, 0))[0] for k in NEAREST[:5]} <= set(done_groups[0]) and state["gate"] == 0:
+                landed(what)
+            for i in groups[what]:
+                half, lands = items[i][4:6]
+                key_ = (chunk, spot(lands)[0])
+                held[key_] = held.get(key_, 0.0) + (1.0 if half is None else 0.5)
+                if held[key_] == (6.0 if spot(lands)[0] == 0 else 8.0):
+                    done_groups[chunk].append(spot(lands)[0])
+            for k in done_groups[0][state["gate"] :]:
                 with jax.named_scope("gu_a"):
-                    gate_up(tok, every, 0, 5)
-                state["gate"] = 5
-            if chunk == 0 and len(done_groups[0]) == NZ and state["gate"] == 5:
-                with jax.named_scope("gu_b"):
-                    gate_up(tok, every, 5, 8)
-                    hidden(every)
-                state["gate"] = 8
-            if state["gate"] == 8:
+                    gate_up(z_at[k])
+                state["gate"] += 1
+                if state["gate"] == NZ:
+                    with jax.named_scope("gu_b"):
+                        hidden(every)
+            if state["gate"] == NZ:
                 for k in done_groups[1]:
                     if k not in state["fronts"]:
                         state["fronts"].append(k)
                         with jax.named_scope("front1"):
                             first_front(z_at[k])
                         state["middles"].append(z_at[k])
-                        flush_middles(2)
-                if len(state["fronts"]) == NZ:
-                    flush_middles(0)
+        elif kind == "middles":
+            flush_middles(what)
         elif kind == "settle":
             def store_first(normed):
-                first[pl.ds(row0, OWN), :] = normed
+                for half in range(2):
+                    first[half, pl.ds(pl.multiple_of(tp * 16, 16), 16), :] = normed[16 * half : 16 * half + 16]
             with jax.named_scope("settle1"):
                 settle(tok[pl.ds(row0, OWN), :], store_first, 0.5, 0, None)
             spread_out(first, 0)
             spread_out(first, 1)
         else:
             with jax.named_scope("pass1"):
-                pass_on(first, *what)
-    with jax.named_scope("gathered1"):
-        gathered(first, 0)
-        gathered(first, 1)
-
-    with jax.named_scope("proj"):
-        rows = first[...]
-        pieces = [dot_nn(rows, QA[...].reshape(D, cuts[2]))]
-        if cuts[2] < 384:
-            pieces.append(dot_nn(rows, QB[:, :, :, : 384 - cuts[2]].reshape(D, 384 - cuts[2])))
-        proj = jnp.concatenate(pieces, axis=1)
-        ranks = dot_nt(rows, rank_down[...])
+                pass_all(first, what)
+
+    for half in range(2):
+        with jax.named_scope("gathered1"):
+            gathered(first, half)
+        with jax.named_scope("proj"):
+            rows = first[half]
+            pieces = [dot_nn(rows, QA[...].reshape(D, cuts[2]))]
+            if cuts[2] < 384:
+                pieces.append(dot_nn(rows, QB[:, :, : 384 - cuts[2]].reshape(D, 384 - cuts[2])))
+            pieces.append(dot_nt(rows, rank_down[...]))
+            at = 0
+            for piece in pieces:
+                wide = piece.shape[1]
+                for t in range(8):
+                    projected[t * OWN + 16 * half : t * OWN + 16 * half + 16, at : at + wide] = piece[t * 16 : t * 16 + 16]
+                at += wide
+    with jax.named_scope("decay"):
+        ranks = projected[:, 384:400]
         pair_at = pl.multiple_of(x * 128, 128)
 
         def mine(ref):
@@ -457,14 +480,16 @@
         source = dot_nn(ranks, mine(rank_up), lax.Precision.HIGHEST) + mine(bias)
         log_decay = (jnp.minimum(source, 0.0) - jnp.log1p(jnp.exp(-jnp.abs(source)))) * (1.0 / GATE_SOFTNESS)
     with jax.named_scope("gla"):
-        heads = head_out(proj[:, :DK] * DK**-0.5, proj[:, DK : 2 * DK], proj[:, 128:256], log_decay)
+        heads = head_out(projected[:, :DK] * DK**-0.5, projected[:, DK : 2 * DK], projected[:, 128:256], log_decay)
         scale = lax.rsqrt(jnp.mean(heads * heads, axis=1, keepdims=True) + HEAD_FLOOR)
         gain = head_gain[:, pl.ds(pl.multiple_of(tp * DV, DV), DV)]
-        mixed[...] = (heads * scale * gain * silu(proj[:, 256:384])).astype(BF16)
+        mixed[...] = (heads * scale * gain * silu(projected[:, 256:384])).astype(BF16)
     drain_sums(None)
+    for half in range(2):
+        drain_rows(half)
 
     def output_fronts(k):
-        part = dot_nt(mixed[...], QB[4 * k : 4 * k + 4, :, :, -128:].reshape(4 * COLS, 128))
+        part = dot_nt(mixed[...], group_of(QB, 4 * k, 4)[:, -128:])
         for g in range(4):
             for t in range(8):
                 sendbuf[4 * k + g, t % 2, t // 2] = part[
@@ -485,18 +510,13 @@
         middles(0, 0, 4)
         middles(1, 0, 4)
 
-    leaving = []
-
-    def put_out(k, half, xx, cc):
-        copy = pltpu.make_async_copy(block(third, xx, cc, half), block(out, xx, cc, half), out_sem.at[k, half])
-        copy.start()
-        leaving.append(copy)
+    def put_out(half, xx, cc):
+        pltpu.make_async_copy(block(third, xx, cc, half), block(out, xx, cc, half), out_sem.at[0]).start()
 
     def settle_second(half):
         def store(normed):
             second[half, pl.ds(pl.multiple_of(tp * 16, 16), 16), :] = normed
-        start = pl.multiple_of(row0 + 16 * half, 16)
-        settle(first[pl.ds(start, 16), :], store, 1.0, 1, half)
+        settle(first[half, pl.ds(pl.multiple_of(tp * 16, 16), 16), :], store, 1.0, 1, half)
         spread_out(second, half)
 
     def settle_last(half):
@@ -504,7 +524,7 @@
             third[pl.ds(pl.multiple_of(row0 + 16 * half, 16), 16), :] = normed
         settle(second[half, pl.ds(pl.multiple_of(tp * 16, 16), 16), :], store, 0.5, 2, half)
         spread_out(third, half)
-        put_out(7, half, x, c)
+        put_out(half, x, c)
 
     def rows_of(half):
         return slice(128 * half, 128 * half + 128)
@@ -518,9 +538,7 @@
     def down_sums(half):
         rows, cut = rows_of(half), cuts[1]
         for k in range(2):
-            groups = slice(4 * k, 4 * k + 4)
-            part = dot_nt(hid[rows, :cut], DA[groups].reshape(4 * COLS, cut)) + dot_nt(
-                hid[rows, cut:], DB[groups].reshape(4 * COLS, 768 - cut))
+            part = dot_nt(hid[rows, :cut], group_of(DA, 4 * k, 4)) + dot_nt(hid[rows, cut:], group_of(DB, 4 * k, 4))
             for g in range(4):
                 for t in range(8):
                     sendbuf[4 * k + g, t % 2, t // 2, 16 * half : 16 * half + 16] = part[
@@ -551,8 +569,7 @@
         drain_sums(1)
         down_sums(1)
     for half in range(2):
-        drain_rows(first, half)
-        drain_rows(second, half)
+        drain_rows(half)
     with jax.named_scope("settle3a"):
         settle_last(0)
     with jax.named_scope("settle3b"):
@@ -561,24 +578,21 @@
         with jax.named_scope("pass3"):
             for s in (0, 2, 1):
                 pass_on(third, s, half)
-                put_out(s, half, from_x[s], c)
+                put_out(half, from_x[s], c)
     with jax.named_scope("puts"):
-        for _, kind, i in order:
-            if kind == "send":
-                item_copy(i, False).wait_send()
+        all_put()
     for half in range(2):
         with jax.named_scope("gathered3"):
             ag_copy(third, 3, half, x, other, partner).wait_recv()
-            put_out(3, half, x, other)
+            put_out(half, x, other)
             for s in (0, 2, 1):
                 ag_copy(third, 4 + s, half, from_x[s], other, partner).wait_recv()
-                put_out(4 + s, half, from_x[s], other)
+                put_out(half, from_x[s], other)
     with jax.named_scope("drain"):
         for half in range(2):
             drain_sums(half)
-            drain_rows(third, half)
-        for copy in leaving:
-            copy.wait()
+            drain_rows(half)
+        pltpu.make_async_copy(third, out, out_sem.at[0]).wait()
 
 
 def per_device(
@@ -589,28 +603,28 @@
         tokens, ffn_gate, ffn_up, ffn_down.T, query_proj, key_proj, value_proj, outgate_proj, output_proj.T,
         rank_down.T, rank_up, decay_bias.reshape(1, -1), head_gain.reshape(1, -1), norm_gain, norm_bias,
     )
-    items, order = gather_order()
-    count = len(items)
+    items, groups, order = gather_order()
     dma = pltpu.SemaphoreType.DMA
     scratch = [pltpu.VMEM(a.shape, a.dtype) for a in operands]
-    scratch += [pltpu.VMEM((NZ, NY, SHARD, tiles * LANES), BF16) for pair in WIDTHS for tiles in pair]
+    scratch += [pltpu.VMEM((NZ * NY, SHARD, tiles * LANES), BF16) for pair in WIDTHS for tiles in pair]
     scratch += [
         pltpu.VMEM((ROWS, 1408), F32),
         pltpu.VMEM((ROWS, 768), BF16),
-        pltpu.VMEM((ROWS, D), BF16),
+        pltpu.VMEM((2, ROWS // 2, D), BF16),
         pltpu.VMEM((2, ROWS // 2, D), BF16),
         pltpu.VMEM((ROWS, D), BF16),
         pltpu.VMEM((ROWS, DV), BF16),
+        pltpu.VMEM((ROWS, 512), F32),
         pltpu.VMEM((NZ, 2, NX, OWN, COLS), BF16),
         pltpu.VMEM((NZ, NX, OWN, COLS), BF16),
         pltpu.VMEM((NZ, NX, OWN, COLS), BF16),
         pltpu.VMEM((3, NZ, OWN, COLS), BF16),
         pltpu.VMEM((OWN, D), F32),
-        dma((count,)), dma((count,)), dma((15,)),
-        dma((2, NZ)), dma((2, NZ)), dma((2, 3, NZ)), dma((2, 3, NZ)), dma((7, 2)), dma((7, 2)), dma((8, 2)),
+        dma((2 * len(WIDTHS),)), dma((len(groups),)), dma((15,)),
+        dma((2,)), dma((NZ,)), dma((2, 3)), dma((2, 3)), dma((2,)), dma((7, 2)), dma((1,)),
     ]
     rows = pl.pallas_call(
-        functools.partial(layer_kernel, items, order),
+        functools.partial(layer_kernel, items, groups, order),
         out_shape=jax.ShapeDtypeStruct((ROWS, D), BF16),
         in_specs=[pl.BlockSpec(memory_space=pltpu.HBM)] * 15,
         out_specs=pl.BlockSpec(memory_space=pltpu.HBM),

time: 128 us -> 123 us (0.961)
  Pallas kernels: 125 us -> 120 us
    pallas_call x1, Pallas kernels: 125 us -> 120 us  [per_device(): pl.pallas_call(functools.partial(layer_kernel, items, groups, order), out...]
where the time goes in v3:
time: 123 us
  Pallas kernels  120 us (98%)
  other arithmetic  2.27 us (2%)
    pallas_call x1, Pallas kernels, per_device(): pl.pallas_call(functools.partial(layer_kernel, items, groups, order), out...  120 us

profile of v3, /device:TPU:1, one launch (start us, length us, event | category | flops | bytes accessed | tf_op | source)
XLA Modules:
  0.0 122.6 jit_solution(17824981549591834527)
XLA Ops:
  0.0 120.4 %layer.1 = bf16[256,2048]{1,0:T(8,128)(2,1)} custom-call(bf16[256,2048]{1,0:T(8,128)(2,1)} %refs_0_.1, bf16[64,704]{1,0:T(8,128)(2,1)} %refs_1_.1, bf16[64,704]{1,0:T(8,128)(2,1)} %refs_2_.1, bf16[64,704]{1,0:T(8,128)(2,1)} %bitcast.5, bf16[64,64]{1,0:T(8,128)(2,1)} %refs_4_.1, bf16[64,64]{1,0:T(8,128)(2,1)} %refs_5_.1, bf16[64,128]{1,0:T(8,128)(2,1)} %refs_6_.1, ...), custom_call_target="tpu_custom_call" | custom-call | tf_op jit(solution)/shard_map/layer/pallas_call | solution.py:626
  120.4 2.3 %broadcast_select_fusion = bf16[256,2048]{1,0:T(8,128)(2,1)} fusion(bf16[256,2048]{1,0:T(8,128)(2,1)} %layer.1, pred[]{:T(512)S(6)} %ge.3), kind=kLoop, calls=%fused_computation | loop fusion | flops 524288 | bytes 2097153 | tf_op jit(solution)/shard_map/jit(_where)/select_n | solution.py:636

commit v4 on v3

--- a/solution.py
+++ b/solution.py
@@ -19,6 +19,7 @@
 SHARD = 64
 COLS = 256
 OWN = 32
+HALF = 128
 LANES = 128
 
 EPSILON = 1e-05
@@ -40,7 +41,7 @@
 BACKLOG = 2.525
 MIDDLES_AT = ((-2.0, 1), (-1.0, 1), (0.0, 1), (1.5, 0))
 SETTLE_AT = 4.5
-PASS_AT = 11.0
+PASS_AT = 10.5
 
 
 def spot(slot):
@@ -50,24 +51,30 @@
 def gather_items():
     items, groups = [], []
 
-    def add(chunk, part, pair, rise):
-        members = []
+    shared = {}
+
+    def add(chunk, part, pair, rise, share=None):
+        if share is None or (chunk, part, share) not in shared:
+            shared[chunk, part, share] = len(groups)
+            groups.append([])
+        group = shared[chunk, part, share]
         for link, slot, half in pair:
             dz, dy = slot
             lands = {"z+": (dz - 1, dy), "z-": (dz + 1, dy), "y+": (dz, dy - 1), "y-": (dz, dy + 1)}[link]
             size = WIDTHS[chunk][part] * (1.0 if half is None else 0.5)
-            members.append(len(items))
-            items.append((chunk, part, link, slot, half, lands, CHUNK_LATE[chunk] - rise, size, len(groups)))
-        groups.append(members)
+            groups[group].append(len(items))
+            items.append((chunk, part, link, slot, half, lands, CHUNK_LATE[chunk] - rise, size, group))
 
     def along_z(chunk, part, dy, rise):
         for s in range(4):
             halves = (None, None) if s < 3 else (0, 1)
-            add(chunk, part, [("z+", (-s, dy), halves[0]), ("z-", (s, dy), halves[1])], rise[s])
+            share = "ends" if part == 1 and s == 3 else None
+            add(chunk, part, [("z+", (-s, dy), halves[0]), ("z-", (s, dy), halves[1])], rise[s], share)
 
     def along_y(chunk, part, dz, rise):
         add(chunk, part, [("y+", (dz, 0), None), ("y-", (dz, 0), None)], rise[0])
-        add(chunk, part, [("y+", (dz, -1), 0), ("y-", (dz, 1), 1)], rise[1])
+        share = None if part == 1 else abs(dz) if chunk < 2 else 0
+        add(chunk, part, [("y+", (dz, -1), 0), ("y-", (dz, 1), 1)], rise[1], share)
 
     for chunk in range(len(WIDTHS)):
         along_z(chunk, 0, 0, FIRST_Z)
@@ -134,30 +141,31 @@
 
 def boundary(prefix, m):
     if m >= 4:
-        parts = prefix.reshape(ROWS // (2 * m), 2 * m, DK)
+        parts = prefix.reshape(HALF // (2 * m), 2 * m, DK)
         edge = jnp.broadcast_to(parts[:, m - 1 : m, :], parts.shape)
-        return edge.reshape(ROWS, DK)
-    parts = prefix.reshape(ROWS // 8, 8, DK)
+        return edge.reshape(HALF, DK)
+    parts = prefix.reshape(HALF // 8, 8, DK)
     row = lax.broadcasted_iota(jnp.int32, parts.shape, 1)
     edge = jnp.broadcast_to(parts[:, 8 - m - 1 : 8 - m, :], parts.shape)
     for at in range(8 - 4 * m, -1, -2 * m):
         edge = jnp.where(row < at + 2 * m, jnp.broadcast_to(parts[:, at + m - 1 : at + m, :], parts.shape), edge)
-    return edge.reshape(ROWS, DK)
+    return edge.reshape(HALF, DK)
 
 
 def head_out(q, k, v, log_decay):
-    row = lax.broadcasted_iota(jnp.int32, (ROWS, ROWS), 0)
-    col = lax.broadcasted_iota(jnp.int32, (ROWS, ROWS), 1)
+    row = lax.broadcasted_iota(jnp.int32, (HALF, HALF), 0)
+    col = lax.broadcasted_iota(jnp.int32, (HALF, HALF), 1)
     prefix = dot_nn((col <= row).astype(F32), log_decay, lax.Precision.HIGHEST)
     apart = row ^ col
-    scores = jnp.where(row == col, jnp.sum(q * k, axis=1, keepdims=True), 0.0)
-    m = ROWS // 2
-    while m:
+    scores = jnp.broadcast_to(jnp.sum(q * k, axis=1, keepdims=True), apart.shape)
+    m = 1
+    while m < HALF:
         fade = jnp.exp(-jnp.abs(prefix - boundary(prefix, m)))
         level = dot_nt((q * fade).astype(BF16), (k * fade).astype(BF16))
-        scores = jnp.where((row > col) & (apart >= m) & (apart < 2 * m), level, scores)
-        m //= 2
-    return dot_nn(scores.astype(BF16), v.astype(BF16))
+        scores = jnp.where(apart >= m, level, scores)
+        m *= 2
+    scores = jnp.where(row >= col, scores, 0.0)
+    return dot_nn(scores.astype(BF16), v.astype(BF16)), prefix
 
 
 def layer_kernel(items, groups, order, *refs):
@@ -250,8 +258,9 @@
             device_id=where["z+"], device_id_type=MESH)
 
     def landed(group):
-        chunk, part, _, _, half = items[groups[group][0]][:5]
-        bytes_of(chunk, part, 2 if half is None else 1, group).wait_recv()
+        chunk, part = items[groups[group][0]][:2]
+        slabs = sum(2 if items[i][4] is None else 1 for i in groups[group]) // 2
+        bytes_of(chunk, part, slabs, group).wait_recv()
 
     def all_put():
         for chunk in range(len(WIDTHS)):
@@ -346,7 +355,7 @@
         t = xx * 2 + cc
         if target is not third and target is not out:
             return target.at[half, pl.ds(pl.multiple_of(t * 16, 16), 16)]
-        return target.at[pl.ds(pl.multiple_of(t * OWN + 16 * half, 16), 16)]
+        return target.at[pl.ds(pl.multiple_of(t * 16 + HALF * half, 16), 16)]
 
     def ag_copy(target, k, half, xx, cc, to):
         ref = block(target, xx, cc, half)
@@ -388,7 +397,6 @@
             sums_of(half, s).wait_send()
 
     every = slice(0, ROWS)
-    row0 = pl.multiple_of(tp * OWN, OWN)
     held = {}
     done_groups = [[], [], []]
     state = {"gate": 0, "fronts": [], "middles": []}
@@ -396,7 +404,7 @@
     steps = [(t, 0, kind, i) for t, kind, i in order]
     steps += [(end_of[1] + at, 1, "middles", keep) for at, keep in MIDDLES_AT]
     steps += [(end_of[1] + SETTLE_AT, 2, "settle", 0)]
-    steps += [(end_of[1] + PASS_AT + 2.5 * half, 3, "pass", half) for half in range(2)]
+    steps += [(end_of[1] + PASS_AT, 3, "pass", 0)]
     steps.sort(key=lambda e: e[:2])
     clear(every)
     loads[0].wait()
@@ -406,7 +414,9 @@
     def first_front(zi):
         value = down_part(every)(zi)
         for t in range(8):
-            sendbuf[zi, t % 2, t // 2] = value[t * OWN : (t + 1) * OWN].astype(BF16)
+            for half in range(2):
+                at = HALF * half + 16 * t
+                sendbuf[zi, t % 2, t // 2, 16 * half : 16 * half + 16] = value[at : at + 16].astype(BF16)
         pair_copy(zi, None).start()
 
     def flush_middles(keep):
@@ -448,103 +458,118 @@
                 for half in range(2):
                     first[half, pl.ds(pl.multiple_of(tp * 16, 16), 16), :] = normed[16 * half : 16 * half + 16]
             with jax.named_scope("settle1"):
-                settle(tok[pl.ds(row0, OWN), :], store_first, 0.5, 0, None)
+                own_rows = [tok[pl.ds(pl.multiple_of(tp * 16 + HALF * half, 16), 16), :] for half in range(2)]
+                settle(jnp.concatenate([a.astype(F32) for a in own_rows], axis=0), store_first, 0.5, 0, None)
             spread_out(first, 0)
             spread_out(first, 1)
         else:
             with jax.named_scope("pass1"):
                 pass_all(first, what)
 
-    for half in range(2):
-        with jax.named_scope("gathered1"):
-            gathered(first, half)
-        with jax.named_scope("proj"):
-            rows = first[half]
-            pieces = [dot_nn(rows, QA[...].reshape(D, cuts[2]))]
-            if cuts[2] < 384:
-                pieces.append(dot_nn(rows, QB[:, :, : 384 - cuts[2]].reshape(D, 384 - cuts[2])))
-            pieces.append(dot_nt(rows, rank_down[...]))
-            at = 0
-            for piece in pieces:
-                wide = piece.shape[1]
-                for t in range(8):
-                    projected[t * OWN + 16 * half : t * OWN + 16 * half + 16, at : at + wide] = piece[t * 16 : t * 16 + 16]
-                at += wide
-    with jax.named_scope("decay"):
-        ranks = projected[:, 384:400]
-        pair_at = pl.multiple_of(x * 128, 128)
-
-        def mine(ref):
-            both = ref[:, pl.ds(pair_at, 128)].astype(F32)
-            return jnp.where(c == 0, both[:, :64], both[:, 64:])
+    pair_at = pl.multiple_of(x * 128, 128)
+
+    def mine(ref):
+        both = ref[:, pl.ds(pair_at, 128)].astype(F32)
+        return jnp.where(c == 0, both[:, :64], both[:, 64:])
+
+    def rows_of(half):
+        return slice(HALF * half, HALF * half + HALF)
+
+    def project(half):
+        rows = first[half]
+        projected[rows_of(half), : cuts[2]] = dot_nn(rows, QA[...].reshape(D, cuts[2]))
+        if cuts[2] < 384:
+            projected[rows_of(half), cuts[2] : 384] = dot_nn(rows, QB[:, :, : 384 - cuts[2]].reshape(D, 384 - cuts[2]))
+        ranks = dot_nt(rows, rank_down[...])
         source = dot_nn(ranks, mine(rank_up), lax.Precision.HIGHEST) + mine(bias)
-        log_decay = (jnp.minimum(source, 0.0) - jnp.log1p(jnp.exp(-jnp.abs(source)))) * (1.0 / GATE_SOFTNESS)
-    with jax.named_scope("gla"):
-        heads = head_out(projected[:, :DK] * DK**-0.5, projected[:, DK : 2 * DK], projected[:, 128:256], log_decay)
+        return (jnp.minimum(source, 0.0) - jnp.log1p(jnp.exp(-jnp.abs(source)))) * (1.0 / GATE_SOFTNESS)
+
+    def attend(half, log_decay, before):
+        rows = rows_of(half)
+        q = projected[rows, :DK] * DK**-0.5
+        k = projected[rows, DK : 2 * DK]
+        v = projected[rows, 128:256]
+        heads, prefix = head_out(q, k, v, log_decay)
+        if before is not None:
+            late = jnp.exp(-jnp.abs(before - before[HALF - 1 : HALF, :]))
+            across = dot_nt(
+                (q * jnp.exp(-jnp.abs(prefix))).astype(BF16), (projected[0:HALF, DK : 2 * DK] * late).astype(BF16))
+            heads = heads + dot_nn(across.astype(BF16), projected[0:HALF, 128:256].astype(BF16))
         scale = lax.rsqrt(jnp.mean(heads * heads, axis=1, keepdims=True) + HEAD_FLOOR)
         gain = head_gain[:, pl.ds(pl.multiple_of(tp * DV, DV), DV)]
-        mixed[...] = (heads * scale * gain * silu(projected[:, 256:384])).astype(BF16)
-    drain_sums(None)
-    for half in range(2):
-        drain_rows(half)
-
-    def output_fronts(k):
-        part = dot_nt(mixed[...], group_of(QB, 4 * k, 4)[:, -128:])
-        for g in range(4):
-            for t in range(8):
-                sendbuf[4 * k + g, t % 2, t // 2] = part[
-                    t * OWN : (t + 1) * OWN, g * COLS : (g + 1) * COLS].astype(BF16)
-        for half in range(2):
-            for g in range(0, 4, 2):
-                pair_copy(4 * k + g, half).start()
-
-    def middles(half, lo, hi):
-        def step(k, carry):
-            middle(2 * k, half)
-            return carry
-        lax.fori_loop(lo, hi, step, 0)
-
-    with jax.named_scope("rs2"):
-        output_fronts(0)
-        output_fronts(1)
-        middles(0, 0, 4)
-        middles(1, 0, 4)
-
-    def put_out(half, xx, cc):
-        pltpu.make_async_copy(block(third, xx, cc, half), block(out, xx, cc, half), out_sem.at[0]).start()
-
-    def settle_second(half):
-        def store(normed):
-            second[half, pl.ds(pl.multiple_of(tp * 16, 16), 16), :] = normed
-        settle(first[half, pl.ds(pl.multiple_of(tp * 16, 16), 16), :], store, 1.0, 1, half)
-        spread_out(second, half)
-
-    def settle_last(half):
-        def store(normed):
-            third[pl.ds(pl.multiple_of(row0 + 16 * half, 16), 16), :] = normed
-        settle(second[half, pl.ds(pl.multiple_of(tp * 16, 16), 16), :], store, 0.5, 2, half)
-        spread_out(third, half)
-        put_out(half, x, c)
-
-    def rows_of(half):
-        return slice(128 * half, 128 * half + 128)
-
-    def mixer_front(half):
-        rows = rows_of(half)
-        acc[rows, : cuts[0]] = dot_nn(second[half], GA[...].reshape(D, cuts[0]))
-        acc[rows, cuts[0] :] = dot_nn(second[half], GB[...].reshape(D, 1408 - cuts[0]))
-        hidden(rows)
-
-    def down_sums(half):
-        rows, cut = rows_of(half), cuts[1]
+        mixed[rows, :] = (heads * scale * gain * silu(projected[rows, 256:384])).astype(BF16)
+        return prefix
+
+    def fronts(half, product):
         for k in range(2):
-            part = dot_nt(hid[rows, :cut], group_of(DA, 4 * k, 4)) + dot_nt(hid[rows, cut:], group_of(DB, 4 * k, 4))
+            part = product(4 * k)
             for g in range(4):
                 for t in range(8):
                     sendbuf[4 * k + g, t % 2, t // 2, 16 * half : 16 * half + 16] = part[
                         t * 16 : (t + 1) * 16, g * COLS : (g + 1) * COLS].astype(BF16)
             for g in range(0, 4, 2):
                 pair_copy(4 * k + g, half).start()
+
+    def output_product(half):
+        return lambda zi: dot_nt(mixed[rows_of(half), :], group_of(QB, zi, 4)[:, -128:])
+
+    def down_product(half):
+        rows, cut = rows_of(half), cuts[1]
+        return lambda zi: dot_nt(hid[rows, :cut], group_of(DA, zi, 4)) + dot_nt(hid[rows, cut:], group_of(DB, zi, 4))
+
+    def middles(half, lo, hi):
+        def step(k, carry):
+            middle(2 * k, half)
+            return carry
+        lax.fori_loop(lo, hi, step, 0)
+
+    with jax.named_scope("gathered1a"):
+        gathered(first, 0)
+    with jax.named_scope("gla_a"):
+        before = attend(0, project(0), None)
+    with jax.named_scope("pass1b"):
+        pass_all(first, 1)
+    with jax.named_scope("rs2a"):
+        drain_sums(None)
+        fronts(0, output_product(0))
+    with jax.named_scope("mid2a"):
+        middles(0, 0, 4)
+    with jax.named_scope("gathered1b"):
+        gathered(first, 1)
+    with jax.named_scope("proj_b"):
+        decay_b = project(1)
+    with jax.named_scope("gla_b"):
+        attend(1, decay_b, before)
+    with jax.named_scope("rs2b"):
+        fronts(1, output_product(1))
+        for half in range(2):
+            drain_rows(half)
+        middles(1, 0, 4)
+
+    def put_out(half, xx, cc):
+        pltpu.make_async_copy(block(third, xx, cc, half), block(out, xx, cc, half), out_sem.at[0]).start()
+
+    def settle_second(half):
+        def store(normed):
+            second[half, pl.ds(pl.multiple_of(tp * 16, 16), 16), :] = normed
+        settle(first[half, pl.ds(pl.multiple_of(tp * 16, 16), 16), :], store, 1.0, 1, half)
+        spread_out(second, half)
+
+    def settle_last(half):
+        def store(normed):
+            third[pl.ds(pl.multiple_of(tp * 16 + HALF * half, 16), 16), :] = normed
+        settle(second[half, pl.ds(pl.multiple_of(tp * 16, 16), 16), :], store, 0.5, 2, half)
+        spread_out(third, half)
+        put_out(half, x, c)
+
+    def mixer_front(half):
+        rows = rows_of(half)
+        acc[rows, : cuts[0]] = dot_nn(second[half], GA[...].reshape(D, cuts[0]))
+        acc[rows, cuts[0] :] = dot_nn(second[half], GB[...].reshape(D, 1408 - cuts[0]))
+        hidden(rows)
+
+    def down_sums(half):
+        fronts(half, down_product(half))
         middles(half, 0, 4)
 
     with jax.named_scope("settle2a"):

time: 123 us -> 120 us (0.976)
  Pallas kernels: 120 us -> 118 us
    pallas_call x1, Pallas kernels: 120 us -> 118 us  [per_device(): pl.pallas_call(functools.partial(layer_kernel, items, groups, order), out...]
where the time goes in v4:
time: 120 us
  Pallas kernels  118 us (98%)
  other arithmetic  2.27 us (2%)
    pallas_call x1, Pallas kernels, per_device(): pl.pallas_call(functools.partial(layer_kernel, items, groups, order), out...  118 us

profile of v4, /device:TPU:1, one launch (start us, length us, event | category | flops | bytes accessed | tf_op | source)
XLA Modules:
  0.0 120.1 jit_solution(18260473278115352627)
XLA Ops:
  0.0 117.8 %layer.1 = bf16[256,2048]{1,0:T(8,128)(2,1)} custom-call(bf16[256,2048]{1,0:T(8,128)(2,1)} %refs_0_.1, bf16[64,704]{1,0:T(8,128)(2,1)} %refs_1_.1, bf16[64,704]{1,0:T(8,128)(2,1)} %refs_2_.1, bf16[64,704]{1,0:T(8,128)(2,1)} %bitcast.5, bf16[64,64]{1,0:T(8,128)(2,1)} %refs_4_.1, bf16[64,64]{1,0:T(8,128)(2,1)} %refs_5_.1, bf16[64,128]{1,0:T(8,128)(2,1)} %refs_6_.1, ...), custom_call_target="tpu_custom_call" | custom-call | tf_op jit(solution)/shard_map/layer/pallas_call | solution.py:651
  117.8 2.3 %broadcast_select_fusion = bf16[256,2048]{1,0:T(8,128)(2,1)} fusion(bf16[256,2048]{1,0:T(8,128)(2,1)} %layer.1, pred[]{:T(512)S(6)} %ge.3), kind=kLoop, calls=%fused_computation | loop fusion | flops 524288 | bytes 2097153 | tf_op jit(solution)/shard_map/jit(_where)/select_n | solution.py:661
